TPU v7x, 32 devices: a whole 2x2x4 slice. The times are simulated.
32 devices in a mesh: rep: 2 (over x), fs: 8 (over z, y), tp: 2 (over core).
Axes of the slice: x: 2, y: 2, z: 4, core: 2. Of those that a mesh axis runs over, the one named last changes fastest.
Arguments:
- tokens: bfloat16 [6144, 2048], P(('rep', 'fs'), 'tp'), may hold values from -6 to 6
- mixing_norm_gain: float32 [2048], replicated, may hold values from 0.1 to 1.9
- recurrent_input_weight: float32 [2048, 3072], P('fs', 'tp'), may hold values from -0.125 to 0.125
- recurrent_input_scale: float32 [3072], P('tp'), may hold values from 0.5 to 2
- convolution_kernel_taps: float32 [4, 3072], P(None, 'tp'), may hold values from -3 to 3
- recurrence_gate_weight_blocks: bfloat16 [24, 128, 128], P('tp'), may hold values from -0.5 to 0.5
- input_gate_weight_blocks: bfloat16 [24, 128, 128], P('tp'), may hold values from -0.5 to 0.5
- channel_decay_parameter: float32 [3072], P('tp'), may hold values from 3 to 9
- token_extra_log_decay: float32 [6144], P(('rep', 'fs')), may hold values from -0.7 to 0
- mixing_output_weight: float32 [3072, 2048], P('tp', 'fs'), may hold values from -0.109375 to 0.109375
- mixing_output_scale: float32 [2048], P('fs'), may hold values from 0.5 to 2
- feedforward_norm_gain: float32 [2048], replicated, may hold values from 0.1 to 1.9
- feedforward_gate_weight: float32 [2048, 5120], P('fs', 'tp'), may hold values from -0.125 to 0.125
- feedforward_gate_scale: float32 [5120], P('tp'), may hold values from 0.5 to 2
- feedforward_up_weight: float32 [2048, 5120], P('fs', 'tp'), may hold values from -0.125 to 0.125
- feedforward_up_scale: float32 [5120], P('tp'), may hold values from 0.5 to 2
- feedforward_down_weight: float32 [5120, 2048], P('tp', 'fs'), may hold values from -0.078125 to 0.078125
- feedforward_down_scale: float32 [2048], P('fs'), may hold values from 0.5 to 2
Outputs:
- layer_out: bfloat16 [6144, 2048], P(('rep', 'fs'), 'tp')
All inputs are finite; a program needn't handle non-finite values.
Results may differ from a plain program's by a relative error of at most 0.02.
Values may be sent and summed in bfloat16 or wider, within the bound.
A program may use at most 128 MiB of HBM per device.

v0:
```python
import jax
import jax.numpy as jnp
from jax import lax
from jax.experimental import pallas as pl
from jax.experimental.pallas import tpu as pltpu
from jax.sharding import PartitionSpec as P

EPS = 1e-06
DECAY_FACTOR = 8.0


def row_norm(rows, gain_vec):
    values = rows.astype(jnp.float32)
    inverse = lax.rsqrt(jnp.mean(values * values, axis=-1, keepdims=True) + EPS)
    return (values * inverse * gain_vec).astype(jnp.bfloat16)


def gather_normed(rows, gain_vec):
    whole_rows = lax.all_gather(rows, "tp", axis=1, tiled=True)
    return row_norm(whole_rows, gain_vec)


def share_sums(terms):
    return lax.psum_scatter(
        terms.astype(jnp.bfloat16), "tp", scatter_dimension=1, tiled=True
    ).astype(jnp.float32)


def combine_pairs(earlier, later):
    decay_one, value_one = earlier
    decay_two, value_two = later
    return (decay_one * decay_two, decay_two * value_one + value_two)


def add_one(left_rows, weight_piece):
    return jnp.dot(left_rows, weight_piece, preferred_element_type=jnp.float32)


def place_columns(left_rows, total_now, pieces, start_row):
    weight_piece, scale_piece = pieces
    product = jnp.dot(left_rows, weight_piece, preferred_element_type=jnp.float32) * scale_piece
    return lax.dynamic_update_slice_in_dim(total_now, product, start_row, 1)


def plain_body(
    tokens,
    mixing_norm_gain,
    recurrent_input_weight,
    recurrent_input_scale,
    convolution_kernel_taps,
    recurrence_gate_weight_blocks,
    input_gate_weight_blocks,
    channel_decay_parameter,
    token_extra_log_decay,
    mixing_output_weight,
    mixing_output_scale,
    feedforward_norm_gain,
    feedforward_gate_weight,
    feedforward_gate_scale,
    feedforward_up_weight,
    feedforward_up_scale,
    feedforward_down_weight,
    feedforward_down_scale,
):
    normed = gather_normed(tokens, mixing_norm_gain)
    seq_rows = normed.shape[0]
    model_width = normed.shape[1]
    width_dev = recurrent_input_weight.shape[1]
    rec_sum = add_one(
        normed,
        lax.all_gather(recurrent_input_weight.astype(jnp.bfloat16), "fs", axis=0, tiled=True),
    )
    rec_input = (rec_sum * recurrent_input_scale).astype(jnp.bfloat16)
    rec_f32 = rec_input.astype(jnp.float32)
    tap_count = convolution_kernel_taps.shape[0]
    padded = jnp.pad(rec_f32, ((tap_count - 1, 0), (0, 0)))
    conv_out = jnp.zeros((seq_rows, width_dev), jnp.float32)
    for tap_index in range(tap_count):
        conv_out = (
            conv_out + convolution_kernel_taps[tap_index] * padded[tap_index : tap_index + seq_rows]
        )
    block_count = recurrence_gate_weight_blocks.shape[0]
    block_size = recurrence_gate_weight_blocks.shape[1]
    blocks = conv_out.astype(jnp.bfloat16).reshape(seq_rows, block_count, block_size)
    recurrence_gate_values = jax.nn.sigmoid(
        jnp.einsum(
            "lni,nij->lnj",
            blocks,
            recurrence_gate_weight_blocks,
            preferred_element_type=jnp.float32,
        ).reshape(seq_rows, width_dev)
    )
    input_gate = jax.nn.sigmoid(
        jnp.einsum(
            "lni,nij->lnj", blocks, input_gate_weight_blocks, preferred_element_type=jnp.float32
        ).reshape(seq_rows, width_dev)
    )
    decay_logarithm = (
        -DECAY_FACTOR * recurrence_gate_values * jax.nn.softplus(-channel_decay_parameter)
        + token_extra_log_decay[:, None]
    )
    decay = jnp.exp(decay_logarithm)
    drive = jnp.sqrt(-jnp.expm1(2.0 * decay_logarithm)) * input_gate * conv_out
    _, state = lax.associative_scan(combine_pairs, (decay, drive), axis=0)
    state_low = state.astype(jnp.bfloat16)
    mix_terms = place_columns(
        state_low,
        jnp.zeros((seq_rows, model_width), jnp.float32),
        (
            lax.all_gather(mixing_output_weight.astype(jnp.bfloat16), "fs", axis=1, tiled=True),
            lax.all_gather(
                mixing_output_scale.reshape(1, -1).astype(jnp.bfloat16), "fs", axis=1, tiled=True
            ).astype(jnp.float32),
        ),
        jnp.int32(0),
    )
    mixed = (tokens.astype(jnp.float32) + share_sums(mix_terms)).astype(jnp.bfloat16)
    normed_ffn = gather_normed(mixed, feedforward_norm_gain)
    gate_sum = add_one(
        normed_ffn,
        lax.all_gather(feedforward_gate_weight.astype(jnp.bfloat16), "fs", axis=0, tiled=True),
    )
    up_sum = add_one(
        normed_ffn,
        lax.all_gather(feedforward_up_weight.astype(jnp.bfloat16), "fs", axis=0, tiled=True),
    )
    hidden = (
        jax.nn.silu(gate_sum * feedforward_gate_scale) * (up_sum * feedforward_up_scale)
    ).astype(jnp.bfloat16)
    down_terms = place_columns(
        hidden,
        jnp.zeros((seq_rows, model_width), jnp.float32),
        (
            lax.all_gather(feedforward_down_weight.astype(jnp.bfloat16), "fs", axis=1, tiled=True),
            lax.all_gather(
                feedforward_down_scale.reshape(1, -1).astype(jnp.bfloat16), "fs", axis=1, tiled=True
            ).astype(jnp.float32),
        ),
        jnp.int32(0),
    )
    return (mixed.astype(jnp.float32) + share_sums(down_terms)).astype(jnp.bfloat16)


REC, MIX, GU, DOWN = range(4)
LOW = jnp.bfloat16
F32 = jnp.float32


def remote(src, dst, send_sem, recv_sem, device):
    return pltpu.make_async_remote_copy(
        src_ref=src,
        dst_ref=dst,
        send_sem=send_sem,
        recv_sem=recv_sem,
        device_id=device,
        device_id_type=pl.DeviceIdType.MESH,
    )


def layer_kernel(
    tokens,
    w_rec,
    w_mix,
    w_gate,
    w_up,
    w_down,
    gain_one,
    rec_scale,
    taps,
    recur_blocks,
    input_blocks,
    decay_param,
    extra,
    mix_scale,
    gain_two,
    gate_scale,
    up_scale,
    down_scale,
    out,
    nbuf,
    rec_w,
    mix_w,
    gu_w,
    down_w,
    f_rec,
    f_mix,
    f_gu,
    f_down,
    y_rec,
    y_mix,
    y_gu,
    y_down,
    tk,
    mx,
    st,
    hid,
    ri,
    ext,
    ecol,
    oth,
    kept,
    rt,
    r1,
    r2,
    oo,
    ob,
    load_sem,
    out_sem,
    wy_send,
    wo_send,
    wf_send,
    w_recv,
    g_send,
    g_recv,
    tt_sem,
    ex_send,
    ex_recv,
    m_send,
    m_recv,
    o_send,
    o_recv,
):
    rows, half_width = tokens.shape
    half, part = rows // 2, rows // 4
    width = half_width * 2
    chans = rec_w.shape[2]
    units = down_w.shape[1]
    cols = mix_w.shape[2]
    block = recur_blocks.shape[1]
    tap_count = taps.shape[0]

    r, f, t = lax.axis_index("rep"), lax.axis_index("fs"), lax.axis_index("tp")
    y, z = lax.rem(f, 2), lax.div(f, 2)
    fp = f + 1 - 2 * y
    q = r * 2 + y
    own, own_x, own_y, own_d = q, (1 - r) * 2 + y, r * 2 + 1 - y, (1 - r) * 2 + 1 - y
    x_dev, y_dev, t_dev = {"rep": 1 - r}, {"fs": fp}, {"tp": 1 - t}
    d_dev = {"rep": 1 - r, "fs": fp}
    inner = lax.div(z + 1, 2) == 1
    near = (1 + lax.rem(z, 2), lax.rem(2 + 3 * z, 5))
    near = tuple({"fs": plane * 2 + y} for plane in near)
    planes = (z, z + 1 - 2 * lax.rem(z, 2), z + 2 - 4 * lax.div(z, 2), 3 - z)
    mats = (rec_w, mix_w, gu_w, down_w)
    top, low = pl.ds(0, part), pl.ds(part, part)

    quarters = (q, r * 2 + 1 - y)
    loads = {}

    def load(name, number, src, dst):
        copy = pltpu.make_async_copy(src, dst, load_sem.at[number])
        copy.start()
        loads[name] = copy

    mine = pl.ds(pl.multiple_of(t * half, half), half)
    theirs = pl.ds(pl.multiple_of((1 - t) * half, half), half)
    side = pl.ds(pl.multiple_of(t * half_width, half_width), half_width)
    load("tok", 0, tokens.at[mine, :], tk.at[:, side])
    for i, piece in enumerate(quarters):
        at = pl.ds(pl.multiple_of(piece * chans, chans), chans)
        load(("rec", i), 1 + i, w_rec.at[:, at], f_rec.at[i])
    for i, piece in enumerate(quarters):
        at = pl.ds(pl.multiple_of(piece * chans, chans), chans)
        load(("mix", i), 3 + i, w_mix.at[at, :], f_mix.at[i])
    for i, piece in enumerate(quarters):
        at = pl.ds(pl.multiple_of(piece * units, units), units)
        load(("gate", i), 5 + i, w_gate.at[:, at], f_gu.at[i, 0])
        load(("up", i), 7 + i, w_up.at[:, at], f_gu.at[i, 1])
        load(("down", i), 9 + i, w_down.at[at, :], f_down.at[i])

    barrier = pltpu.get_barrier_semaphore()
    peers = [x_dev, y_dev, t_dev, d_dev]
    peers += [{"fs": plane * 2 + y} for plane in planes[1:]]
    for device in peers:
        pl.semaphore_signal(barrier, inc=1, device_id=device, device_id_type=pl.DeviceIdType.MESH)
    pl.semaphore_wait(barrier, len(peers))

    token_swap = remote(tokens.at[theirs, :], tk.at[:, side], tt_sem.at[0], tt_sem.at[1], t_dev)
    token_swap.start()

    def block_copy(k, place, send_sem, device):
        view = mats[k].at[place]
        return remote(view, view, send_sem, w_recv.at[k, place], device)

    def wait_block(k, place):
        block_copy(k, place, wo_send.at[0, 0, 0], y_dev).wait_recv()

    def send_own(k, j):
        place = f if j == 0 else fp
        if j == 1:
            wait_block(k, fp)
        for i, device in enumerate(near):
            block_copy(k, place, wo_send.at[k, j, i], device).start()

    y_bufs = (y_rec, y_mix, y_gu, y_down)

    def y_copy(k):
        return remote(y_bufs[k], mats[k].at[f], wy_send.at[k], w_recv.at[k, f], y_dev)

    def forward_copy(k, far, j):
        plane = 3 * (2 - z) if far else 3 - z
        place = plane * 2 + (y if j == 0 else 1 - y)
        edge = 3 * (z - 1)
        return place, block_copy(k, place, wf_send.at[k, far, j], {"fs": edge * 2 + y})

    def forward(k, far, j):
        @pl.when(inner)
        def _():
            place, copy = forward_copy(k, far, j)
            wait_block(k, place)
            copy.start()

    def need(k, p):
        def both():
            wait_block(k, planes[p] * 2)
            wait_block(k, planes[p] * 2 + 1)

        if p == 1:
            both()
        elif p > 1:
            pl.when(jnp.logical_not(inner))(both)

    def norm_rows(src, gain):
        def step(i, carry):
            at = pl.ds(pl.multiple_of(i * 16, 16), 16)
            v = src[at, :].astype(F32)
            inverse = lax.rsqrt(jnp.mean(v * v, axis=-1, keepdims=True) + EPS)
            nbuf[own, t, at, :] = (v * inverse * gain[...]).astype(LOW)
            return carry

        lax.fori_loop(0, half // 16, step, 0)

    def rows_copy(phase, role):
        seq, at, device = (
            (own, top, x_dev),
            (own, low, x_dev),
            (own, top, y_dev),
            (own, low, y_dev),
            (own_y, top, x_dev),
            (own_x, low, y_dev),
            (own, pl.ds(0, half), t_dev),
            (own_x, top, t_dev),
            (own_x, low, t_dev),
            (own_y, top, t_dev),
            (own_y, low, t_dev),
            (own_d, top, t_dev),
            (own_d, low, t_dev),
        )[role]
        view = nbuf.at[seq, t, at, :]
        return remote(view, view, g_send.at[phase, role], g_recv.at[phase, role], device)

    def rows_wait(phase, role):
        seq, side_at, at = (
            (own_x, t, top),
            (own_x, t, low),
            (own_y, t, top),
            (own_y, t, low),
            (own_d, t, top),
            (own_d, t, low),
            (own, 1 - t, pl.ds(0, half)),
            (own_x, 1 - t, top),
            (own_x, 1 - t, low),
            (own_y, 1 - t, top),
            (own_y, 1 - t, low),
            (own_d, 1 - t, top),
            (own_d, 1 - t, low),
        )[role]
        view = nbuf.at[seq, side_at, at, :]
        remote(view, view, g_send.at[phase, role], g_recv.at[phase, role], t_dev).wait_recv()

    def gather_start(phase):
        for role in (1, 2, 0, 3, 6):
            rows_copy(phase, role).start()

    def gather_first(phase):
        rows_wait(phase, 2)
        rows_copy(phase, 4).start()
        rows_wait(phase, 1)
        rows_copy(phase, 5).start()
        rows_copy(phase, 9).start()
        rows_copy(phase, 8).start()

    def gather_second(phase):
        rows_wait(phase, 0)
        rows_copy(phase, 7).start()
        rows_wait(phase, 3)
        rows_copy(phase, 10).start()

    def gather_last(phase):
        rows_wait(phase, 4)
        rows_copy(phase, 11).start()
        rows_wait(phase, 5)
        rows_copy(phase, 12).start()
        for role in range(6, 13):
            rows_wait(phase, role)
        for role in range(13):
            rows_copy(phase, role).wait_send()

    def products(phase, p, left, weights, k):
        need(k, p)
        first = planes[p] * 2

        def other(s, carry):
            for c in range(2):
                value = jnp.dot(left[s, 1 - t], weights[first + c], preferred_element_type=F32)
                oth[p, s, :, c * cols : (c + 1) * cols] = value.astype(LOW)
            return carry

        def keep(s, carry):
            for c in range(2):
                value = jnp.dot(left[s, t], weights[first + c], preferred_element_type=F32)
                kept[p, lax.div(s, 2), lax.rem(s, 2), :, c * cols : (c + 1) * cols] = value.astype(LOW)
            return carry

        lax.fori_loop(0, 4, other, 0)
        sum_copies(phase, p, 0).start()
        lax.fori_loop(0, 4, keep, 0)

    def sum_copies(phase, p, number):
        src, dst, device = (
            (oth.at[p], rt.at[phase, p], t_dev),
            (kept.at[p, 1 - r, :, top, :], r1.at[phase, p, 0], x_dev),
            (kept.at[p, :, 1 - y, low, :], r1.at[phase, p, 1], y_dev),
            (kept.at[p, r, 1 - y, top, :], r2.at[phase, p, 0], y_dev),
            (kept.at[p, 1 - r, y, low, :], r2.at[phase, p, 1], x_dev),
        )[number]
        return remote(src, dst, m_send.at[phase, p, number], m_recv.at[phase, p, number], device)

    def pair_sums(phase, p):
        sum_copies(phase, p, 0).wait_recv()

        def step(s, carry):
            a, b = lax.div(s, 2), lax.rem(s, 2)
            value = kept[p, a, b].astype(F32) + rt[phase, p, s].astype(F32)
            kept[p, a, b] = value.astype(LOW)
            return carry

        lax.fori_loop(0, 4, step, 0)
        sum_copies(phase, p, 1).start()
        sum_copies(phase, p, 2).start()

    def line_sums(phase, p):
        sum_copies(phase, p, 1).wait_recv()
        for i in range(2):
            value = kept[p, r, i, 0:part, :].astype(F32) + r1[phase, p, 0, i].astype(F32)
            kept[p, r, i, 0:part, :] = value.astype(LOW)
        sum_copies(phase, p, 3).start()
        sum_copies(phase, p, 2).wait_recv()
        for i in range(2):
            value = kept[p, i, y, part:half, :].astype(F32) + r1[phase, p, 1, i].astype(F32)
            kept[p, i, y, part:half, :] = value.astype(LOW)
        sum_copies(phase, p, 4).start()

    def last_sums(phase, p, base):
        at = pl.ds(pl.multiple_of(planes[p] * 2 * cols, 2 * cols), 2 * cols)
        values = []
        for i, number in enumerate((3, 4)):
            span = slice(i * part, (i + 1) * part)
            sum_copies(phase, p, number).wait_recv()
            value = kept[p, r, y, span, :].astype(F32) + r2[phase, p, i].astype(F32)
            values.append((base[span, at].astype(F32) + value).astype(LOW))
        for number in range(5):
            sum_copies(phase, p, number).wait_send()
        return at, values

    def mix_done(p):
        at, values = last_sums(0, p, tk)
        for i, value in enumerate(values):
            mx[i * part : (i + 1) * part, at] = value

    def out_copy(p):
        at = pl.ds(pl.multiple_of(lax.rem(planes[p], 2) * 2 * cols, 2 * cols), 2 * cols)
        return remote(oo.at[p], ob.at[t, :, at], o_send.at[p], o_recv.at[p], t_dev)

    def down_done(p):
        _, values = last_sums(1, p, mx)
        local = lax.div(planes[p], 2) == t
        at = pl.ds(pl.multiple_of(lax.rem(planes[p], 2) * 2 * cols, 2 * cols), 2 * cols)

        @pl.when(local)
        def _():
            for i, value in enumerate(values):
                ob[t, i * part : (i + 1) * part, at] = value

        @pl.when(jnp.logical_not(local))
        def _():
            for i, value in enumerate(values):
                oo[p, i * part : (i + 1) * part, :] = value
            out_copy(p).start()

    for i in range(2):
        loads["rec", i].wait()
    y_rec[...] = f_rec[1].astype(LOW)
    rec_w[f] = f_rec[0].astype(LOW)
    y_copy(REC).start()
    send_own(REC, 0)

    ext[own] = jnp.broadcast_to(extra[...], ext.shape[1:])
    loads["tok"].wait()
    token_swap.wait()
    norm_rows(tk, gain_one)
    gather_start(0)
    ext_copies = [
        remote(ext.at[own], ext.at[own], ex_send.at[i], ex_recv.at[i], device)
        for i, device in enumerate((x_dev, y_dev, d_dev))
    ]
    for copy in ext_copies:
        copy.start()

    for i in range(2):
        loads["mix", i].wait()
    y_mix[...] = (f_mix[1] * mix_scale[...]).astype(LOW)
    mix_w[f] = (f_mix[0] * mix_scale[...]).astype(LOW)
    y_copy(MIX).start()
    send_own(MIX, 0)
    send_own(REC, 1)
    for i in range(2):
        for name in ("gate", "up", "down"):
            loads[name, i].wait()
    for i in range(2):
        y_gu[:, i * units : (i + 1) * units] = f_gu[1, i].astype(LOW)
        gu_w[f, :, i * units : (i + 1) * units] = f_gu[0, i].astype(LOW)
    y_down[...] = (f_down[1] * down_scale[...]).astype(LOW)
    down_w[f] = (f_down[0] * down_scale[...]).astype(LOW)

    gather_first(0)
    forward(REC, 0, 0)
    forward(REC, 1, 0)
    send_own(MIX, 1)
    forward(REC, 0, 1)
    forward(REC, 1, 1)
    gather_second(0)
    y_copy(GU).start()
    send_own(GU, 0)
    gather_last(0)
    for i, seq in enumerate((own_x, own_y, own_d)):
        remote(ext.at[seq], ext.at[seq], ex_send.at[i], ex_recv.at[i], t_dev).wait_recv()
    forward(MIX, 0, 0)
    forward(MIX, 0, 1)
    for p in range(1, 4):
        need(REC, p)

    at_chans = pl.multiple_of(q * chans, chans)

    def recur(s, carry):
        left = nbuf[s].reshape(rows, width)
        total = jnp.dot(left, rec_w[...].reshape(width, chans), preferred_element_type=F32)
        ri[...] = (total * rec_scale[:, pl.ds(at_chans, chans)]).astype(LOW)
        ecol[...] = jnp.broadcast_to(ext[s, 0:1, :], (block, rows)).T
        for b in range(chans // block):
            here = slice(b * block, (b + 1) * block)
            lanes = pl.ds(pl.multiple_of(at_chans + b * block, block), block)
            number = q * (chans // block) + b
            values = ri[:, here].astype(F32)
            places = lax.broadcasted_iota(jnp.int32, values.shape, 0)
            conv_out = taps[tap_count - 1 : tap_count, lanes] * values
            for back in range(1, tap_count):
                moved = jnp.where(places >= back, pltpu.roll(values, back, 0), 0.0)
                tap = tap_count - 1 - back
                conv_out = conv_out + taps[tap : tap + 1, lanes] * moved
            conv_low = conv_out.astype(LOW)
            recur_gate = jax.nn.sigmoid(
                jnp.dot(conv_low, recur_blocks[number], preferred_element_type=F32)
            )
            input_gate = jax.nn.sigmoid(
                jnp.dot(conv_low, input_blocks[number], preferred_element_type=F32)
            )
            param = -decay_param[:, lanes]
            soft = jnp.maximum(param, 0.0) + jnp.log1p(jnp.exp(-jnp.abs(param)))
            log_decay = -DECAY_FACTOR * recur_gate * soft + ecol[...]
            decay = jnp.exp(log_decay)
            drive = jnp.sqrt(-jnp.tanh(log_decay) * (1.0 + decay * decay)) * input_gate * conv_out
            step = 1
            while step < rows:
                keep = places >= step
                drive = drive + decay * jnp.where(keep, pltpu.roll(drive, step, 0), 0.0)
                if step * 2 < rows:
                    decay = decay * jnp.where(keep, pltpu.roll(decay, step, 0), 1.0)
                step *= 2
            state = drive.astype(LOW)
            st[s, 0, :, here] = state[:half]
            st[s, 1, :, here] = state[half:]
        return carry

    lax.fori_loop(0, 4, recur, 0)

    forward(MIX, 1, 0)
    forward(MIX, 1, 1)
    send_own(GU, 1)
    y_copy(DOWN).start()
    send_own(DOWN, 0)

    products(0, 0, st, mix_w, MIX)
    products(0, 1, st, mix_w, MIX)
    pair_sums(0, 0)
    products(0, 2, st, mix_w, MIX)
    pair_sums(0, 1)
    line_sums(0, 0)
    products(0, 3, st, mix_w, MIX)
    pair_sums(0, 2)
    line_sums(0, 1)
    mix_done(0)
    pair_sums(0, 3)
    line_sums(0, 2)
    mix_done(1)
    line_sums(0, 3)
    mix_done(2)
    mix_done(3)

    norm_rows(mx, gain_two)
    gather_start(1)
    send_own(DOWN, 1)
    forward(GU, 0, 0)
    gather_first(1)
    forward(GU, 1, 0)
    gather_second(1)
    forward(GU, 0, 1)
    gather_last(1)
    forward(GU, 1, 1)
    for p in range(1, 4):
        need(GU, p)

    at_units = pl.ds(pl.multiple_of(q * units, units), units)

    def hidden(s, carry):
        left = nbuf[s].reshape(rows, width)
        total = jnp.dot(left, gu_w[...].reshape(width, 2 * units), preferred_element_type=F32)
        gate = total[:, :units] * gate_scale[:, at_units]
        up = total[:, units:] * up_scale[:, at_units]
        value = (gate * jax.nn.sigmoid(gate) * up).astype(LOW)
        hid[s, 0] = value[:half]
        hid[s, 1] = value[half:]
        return carry

    lax.fori_loop(0, 4, hidden, 0)

    products(1, 0, hid, down_w, DOWN)
    pair_sums(1, 0)
    forward(DOWN, 0, 0)
    forward(DOWN, 0, 1)
    line_sums(1, 0)
    forward(DOWN, 1, 0)
    forward(DOWN, 1, 1)
    down_done(0)
    for p in range(1, 4):
        products(1, p, hid, down_w, DOWN)
        pair_sums(1, p)
        line_sums(1, p)
        down_done(p)

    for p in range(4):
        local = lax.div(planes[p], 2) == t

        @pl.when(local)
        def _():
            out_copy(p).wait_recv()

        @pl.when(jnp.logical_not(local))
        def _():
            out_copy(p).wait_send()

    result = pltpu.make_async_copy(ob, out, out_sem)
    result.start()
    for k in range(4):
        y_copy(k).wait_send()
        for j in range(2):
            for i, device in enumerate(near):
                block_copy(k, f if j == 0 else fp, wo_send.at[k, j, i], device).wait_send()

        @pl.when(inner)
        def _():
            for far in range(2):
                for j in range(2):
                    forward_copy(k, far, j)[1].wait_send()

    for copy in ext_copies:
        copy.wait_send()
    result.wait()


def team_body(
    tokens,
    mixing_norm_gain,
    recurrent_input_weight,
    recurrent_input_scale,
    convolution_kernel_taps,
    recurrence_gate_weight_blocks,
    input_gate_weight_blocks,
    channel_decay_parameter,
    token_extra_log_decay,
    mixing_output_weight,
    mixing_output_scale,
    feedforward_norm_gain,
    feedforward_gate_weight,
    feedforward_gate_scale,
    feedforward_up_weight,
    feedforward_up_scale,
    feedforward_down_weight,
    feedforward_down_scale,
):
    rows, half_width = tokens.shape
    half, part = rows // 2, rows // 4
    width = half_width * 2
    depth = recurrent_input_weight.shape[0]
    chans = recurrent_input_weight.shape[1] // 4
    units = feedforward_gate_weight.shape[1] // 4
    cols = mixing_output_weight.shape[1]
    block = recurrence_gate_weight_blocks.shape[1]
    planes = width // depth
    any_spec = pl.BlockSpec(memory_space=pl.ANY)
    vmem_spec = pl.BlockSpec(memory_space=pltpu.VMEM)
    vmem = pltpu.VMEM
    dma = pltpu.SemaphoreType.DMA

    def row(vector):
        return vector.reshape(1, -1)

    out = pl.pallas_call(
        layer_kernel,
        out_shape=jax.ShapeDtypeStruct((2, half, half_width), LOW),
        in_specs=[any_spec] * 6 + [vmem_spec] * 12,
        out_specs=any_spec,
        scratch_shapes=[
            vmem((4, 2, half, width), LOW),
            vmem((planes, depth, chans), LOW),
            vmem((planes, chans, cols), LOW),
            vmem((planes, depth, 2 * units), LOW),
            vmem((planes, units, cols), LOW),
            vmem((2, depth, chans), F32),
            vmem((2, chans, cols), F32),
            vmem((2, 2, depth, units), F32),
            vmem((2, units, cols), F32),
            vmem((depth, chans), LOW),
            vmem((chans, cols), LOW),
            vmem((depth, 2 * units), LOW),
            vmem((units, cols), LOW),
            vmem((half, width), LOW),
            vmem((half, width), LOW),
            vmem((4, 2, half, chans), LOW),
            vmem((4, 2, half, units), LOW),
            vmem((rows, chans), LOW),
            vmem((4, 8, rows), F32),
            vmem((rows, block), F32),
            vmem((4, 4, half, 2 * cols), LOW),
            vmem((4, 2, 2, half, 2 * cols), LOW),
            vmem((2, 4, 4, half, 2 * cols), LOW),
            vmem((2, 4, 2, 2, part, 2 * cols), LOW),
            vmem((2, 4, 2, part, 2 * cols), LOW),
            vmem((4, half, 2 * cols), LOW),
            vmem((2, half, half_width), LOW),
            dma((11,)),
            dma,
            dma((4,)),
            dma((4, 2, 2)),
            dma((4, 2, 2)),
            dma((4, planes)),
            dma((2, 13)),
            dma((2, 13)),
            dma((2,)),
            dma((3,)),
            dma((3,)),
            dma((2, 4, 5)),
            dma((2, 4, 5)),
            dma((4,)),
            dma((4,)),
        ],
        compiler_params=pltpu.CompilerParams(
            collective_id=0, has_side_effects=True, vmem_limit_bytes=VMEM_BYTES
        ),
    )(
        tokens,
        recurrent_input_weight,
        mixing_output_weight,
        feedforward_gate_weight,
        feedforward_up_weight,
        feedforward_down_weight,
        row(mixing_norm_gain),
        row(recurrent_input_scale),
        convolution_kernel_taps,
        recurrence_gate_weight_blocks,
        input_gate_weight_blocks,
        row(channel_decay_parameter),
        row(token_extra_log_decay),
        row(mixing_output_scale),
        row(feedforward_norm_gain),
        row(feedforward_gate_scale),
        row(feedforward_up_scale),
        row(feedforward_down_scale),
    )
    return out.reshape(rows, half_width)


VMEM_BYTES = 66_000_000


def team_fits(mesh):
    sizes = mesh.shape
    return sizes["rep"] == 2 and sizes["tp"] == 2 and sizes["fs"] == 8


def solution(mesh):
    placed = (
        P(("rep", "fs"), "tp"),
        P(),
        P("fs", "tp"),
        P("tp"),
        P(None, "tp"),
        P("tp", None, None),
        P("tp", None, None),
        P("tp"),
        P(("rep", "fs")),
        P("tp", "fs"),
        P("fs"),
        P(),
        P("fs", "tp"),
        P("tp"),
        P("fs", "tp"),
        P("tp"),
        P("tp", "fs"),
        P("fs"),
    )

    def body(*args):
        blocks, hidden, rows = args[5].shape[0], args[12].shape[1], args[0].shape[0]
        if not team_fits(mesh) or blocks % 4 or hidden % 512 or rows % 64:
            return plain_body(*args)
        return team_body(*args)

    return jax.shard_map(
        body, mesh=mesh, in_specs=placed, out_specs=P(("rep", "fs"), "tp"), check_vma=False
    )
```

profile of v0, /device:TPU:0, one launch (start us, length us, event | category | flops | bytes accessed | tf_op | source)
XLA Modules:
  0.0 241.0 jit_solution(9389360497335068074)
XLA Ops:
  0.0 1.3 reshape.33.extra
  1.3 1.3 reshape.31.rec_scale
  2.6 1.3 reshape.32.decay_param
  3.8 1.3 reshape.36.gate_scale
  5.2 1.3 reshape.37.up_scale
  6.5 232.4 %shard_map.172 = bf16[2,192,1024]{2,1,0:T(8,128)(2,1)} custom-call(bf16[384,1024]{1,0:T(8,128)(2,1)} %tokens.1, f32[256,1536]{1,0:T(8,128)} %w_rec.1, f32[1536,256]{1,0:T(8,128)} %w_mix.1, f32[256,2560]{1,0:T(8,128)} %w_gate.1, f32[256,2560]{1,0:T(8,128)} %w_up.1, f32[2560,256]{1,0:T(8,128)} %w_down.1, f32[1,2048]{1,0:T(1,128)} %bitcast.6, ...), custom_call_target="tpu_custom_call" | custom-call | tf_op jit(solution)/shard_map/pallas_call | solution.py:717
  238.9 2.1 copy.20
where the time goes:
time: 241 us
  Pallas kernels  232 us (96%)
  local copies, waits for them, and re-layouts  8.52 us (4%)
    pallas_call x1, Pallas kernels, team_body(): pl.pallas_call(layer_kernel, out_shape=jax.ShapeDtypeStruct((2, half, hal...  232 us
    reshape x5, local copies, waits for them, and re-layouts, row(): return vector.reshape(1, -1)  6.46 us

commit v1 on v0

--- a/solution.py
+++ b/solution.py
@@ -272,10 +272,8 @@
     peers += [{"fs": plane * 2 + y} for plane in planes[1:]]
     for device in peers:
         pl.semaphore_signal(barrier, inc=1, device_id=device, device_id_type=pl.DeviceIdType.MESH)
-    pl.semaphore_wait(barrier, len(peers))
 
     token_swap = remote(tokens.at[theirs, :], tk.at[:, side], tt_sem.at[0], tt_sem.at[1], t_dev)
-    token_swap.start()
 
     def block_copy(k, place, send_sem, device):
         view = mats[k].at[place]
@@ -284,12 +282,14 @@
     def wait_block(k, place):
         block_copy(k, place, wo_send.at[0, 0, 0], y_dev).wait_recv()
 
+    def own_place(k, j):
+        return z * 2 + j if k == DOWN else (f if j == 0 else fp)
+
     def send_own(k, j):
-        place = f if j == 0 else fp
-        if j == 1:
+        if j == 1 and k != DOWN:
             wait_block(k, fp)
         for i, device in enumerate(near):
-            block_copy(k, place, wo_send.at[k, j, i], device).start()
+            block_copy(k, own_place(k, j), wo_send.at[k, j, i], device).start()
 
     y_bufs = (y_rec, y_mix, y_gu, y_down)
 
@@ -298,7 +298,7 @@
 
     def forward_copy(k, far, j):
         plane = 3 * (2 - z) if far else 3 - z
-        place = plane * 2 + (y if j == 0 else 1 - y)
+        place = plane * 2 + (j if k == DOWN else (y if j == 0 else 1 - y))
         edge = 3 * (z - 1)
         return place, block_copy(k, place, wf_send.at[k, far, j], {"fs": edge * 2 + y})
 
@@ -309,15 +309,15 @@
             wait_block(k, place)
             copy.start()
 
-    def need(k, p):
-        def both():
-            wait_block(k, planes[p] * 2)
-            wait_block(k, planes[p] * 2 + 1)
+    def need(k, p, blocks=(0, 1)):
+        def wait():
+            for j in blocks:
+                wait_block(k, planes[p] * 2 + j)
 
         if p == 1:
-            both()
+            wait()
         elif p > 1:
-            pl.when(jnp.logical_not(inner))(both)
+            pl.when(jnp.logical_not(inner))(wait)
 
     def norm_rows(src, gain):
         def step(i, carry):
@@ -395,86 +395,94 @@
         for role in range(13):
             rows_copy(phase, role).wait_send()
 
-    def products(phase, p, left, weights, k):
-        need(k, p)
+    def products(phase, p, left, weights, k, blocks=(0, 1)):
+        need(k, p, blocks)
         first = planes[p] * 2
 
-        def other(s, carry):
-            for c in range(2):
-                value = jnp.dot(left[s, 1 - t], weights[first + c], preferred_element_type=F32)
-                oth[p, s, :, c * cols : (c + 1) * cols] = value.astype(LOW)
-            return carry
-
-        def keep(s, carry):
-            for c in range(2):
-                value = jnp.dot(left[s, t], weights[first + c], preferred_element_type=F32)
-                kept[p, lax.div(s, 2), lax.rem(s, 2), :, c * cols : (c + 1) * cols] = value.astype(LOW)
-            return carry
-
-        lax.fori_loop(0, 4, other, 0)
-        sum_copies(phase, p, 0).start()
-        lax.fori_loop(0, 4, keep, 0)
-
-    def sum_copies(phase, p, number):
+        def product(side, c):
+            rows_now = left[:, side].reshape(4 * half, left.shape[-1])
+            value = jnp.dot(rows_now, weights[first + c], preferred_element_type=F32)
+            return value.astype(LOW).reshape(4, half, cols)
+
+        for c in blocks:
+            oth[p, :, :, c * cols : (c + 1) * cols] = product(1 - t, c)
+        sum_copies(phase, p, 0, blocks).start()
+        for c in blocks:
+            value = product(t, c).reshape(2, 2, half, cols)
+            kept[p, :, :, :, c * cols : (c + 1) * cols] = value
+
+    def span_of(blocks):
+        return pl.ds(blocks[0] * cols, len(blocks) * cols)
+
+    def sum_copies(phase, p, number, blocks):
+        at = span_of(blocks)
         src, dst, device = (
-            (oth.at[p], rt.at[phase, p], t_dev),
-            (kept.at[p, 1 - r, :, top, :], r1.at[phase, p, 0], x_dev),
-            (kept.at[p, :, 1 - y, low, :], r1.at[phase, p, 1], y_dev),
-            (kept.at[p, r, 1 - y, top, :], r2.at[phase, p, 0], y_dev),
-            (kept.at[p, 1 - r, y, low, :], r2.at[phase, p, 1], x_dev),
+            (oth.at[p, :, :, at], rt.at[phase, p, :, :, at], t_dev),
+            (kept.at[p, 1 - r, :, top, at], r1.at[phase, p, 0, :, :, at], x_dev),
+            (kept.at[p, :, 1 - y, low, at], r1.at[phase, p, 1, :, :, at], y_dev),
+            (kept.at[p, r, 1 - y, top, at], r2.at[phase, p, 0, :, at], y_dev),
+            (kept.at[p, 1 - r, y, low, at], r2.at[phase, p, 1, :, at], x_dev),
         )[number]
+        number += 5 * blocks[0]
         return remote(src, dst, m_send.at[phase, p, number], m_recv.at[phase, p, number], device)
 
-    def pair_sums(phase, p):
-        sum_copies(phase, p, 0).wait_recv()
+    def pair_sums(phase, p, blocks=(0, 1)):
+        sum_copies(phase, p, 0, blocks).wait_recv()
+        at = span_of(blocks)
 
         def step(s, carry):
             a, b = lax.div(s, 2), lax.rem(s, 2)
-            value = kept[p, a, b].astype(F32) + rt[phase, p, s].astype(F32)
-            kept[p, a, b] = value.astype(LOW)
+            value = kept[p, a, b, :, at].astype(F32) + rt[phase, p, s, :, at].astype(F32)
+            kept[p, a, b, :, at] = value.astype(LOW)
             return carry
 
         lax.fori_loop(0, 4, step, 0)
-        sum_copies(phase, p, 1).start()
-        sum_copies(phase, p, 2).start()
-
-    def line_sums(phase, p):
-        sum_copies(phase, p, 1).wait_recv()
+        sum_copies(phase, p, 1, blocks).start()
+        sum_copies(phase, p, 2, blocks).start()
+
+    def line_sums(phase, p, blocks=(0, 1)):
+        at = span_of(blocks)
+        sum_copies(phase, p, 1, blocks).wait_recv()
         for i in range(2):
-            value = kept[p, r, i, 0:part, :].astype(F32) + r1[phase, p, 0, i].astype(F32)
-            kept[p, r, i, 0:part, :] = value.astype(LOW)
-        sum_copies(phase, p, 3).start()
-        sum_copies(phase, p, 2).wait_recv()
+            value = kept[p, r, i, top, at].astype(F32) + r1[phase, p, 0, i, :, at].astype(F32)
+            kept[p, r, i, top, at] = value.astype(LOW)
+        sum_copies(phase, p, 3, blocks).start()
+        sum_copies(phase, p, 2, blocks).wait_recv()
         for i in range(2):
-            value = kept[p, i, y, part:half, :].astype(F32) + r1[phase, p, 1, i].astype(F32)
-            kept[p, i, y, part:half, :] = value.astype(LOW)
-        sum_copies(phase, p, 4).start()
-
-    def last_sums(phase, p, base):
-        at = pl.ds(pl.multiple_of(planes[p] * 2 * cols, 2 * cols), 2 * cols)
+            value = kept[p, i, y, low, at].astype(F32) + r1[phase, p, 1, i, :, at].astype(F32)
+            kept[p, i, y, low, at] = value.astype(LOW)
+        sum_copies(phase, p, 4, blocks).start()
+
+    def columns_of(plane, blocks):
+        start = pl.multiple_of((plane * 2 + blocks[0]) * cols, cols)
+        return pl.ds(start, len(blocks) * cols)
+
+    def last_sums(phase, p, base, blocks):
+        at, piece = columns_of(planes[p], blocks), span_of(blocks)
         values = []
         for i, number in enumerate((3, 4)):
             span = slice(i * part, (i + 1) * part)
-            sum_copies(phase, p, number).wait_recv()
-            value = kept[p, r, y, span, :].astype(F32) + r2[phase, p, i].astype(F32)
+            sum_copies(phase, p, number, blocks).wait_recv()
+            value = kept[p, r, y, span, piece].astype(F32) + r2[phase, p, i, :, piece].astype(F32)
             values.append((base[span, at].astype(F32) + value).astype(LOW))
         for number in range(5):
-            sum_copies(phase, p, number).wait_send()
+            sum_copies(phase, p, number, blocks).wait_send()
         return at, values
 
     def mix_done(p):
-        at, values = last_sums(0, p, tk)
+        at, values = last_sums(0, p, tk, (0, 1))
         for i, value in enumerate(values):
             mx[i * part : (i + 1) * part, at] = value
 
-    def out_copy(p):
-        at = pl.ds(pl.multiple_of(lax.rem(planes[p], 2) * 2 * cols, 2 * cols), 2 * cols)
-        return remote(oo.at[p], ob.at[t, :, at], o_send.at[p], o_recv.at[p], t_dev)
-
-    def down_done(p):
-        _, values = last_sums(1, p, mx)
+    def out_copy(p, blocks):
+        at = columns_of(lax.rem(planes[p], 2), blocks)
+        src = oo.at[p, :, span_of(blocks)]
+        return remote(src, ob.at[t, :, at], o_send.at[p, blocks[0]], o_recv.at[p, blocks[0]], t_dev)
+
+    def down_done(p, blocks=(0, 1)):
+        _, values = last_sums(1, p, mx, blocks)
         local = lax.div(planes[p], 2) == t
-        at = pl.ds(pl.multiple_of(lax.rem(planes[p], 2) * 2 * cols, 2 * cols), 2 * cols)
+        at = columns_of(lax.rem(planes[p], 2), blocks)
 
         @pl.when(local)
         def _():
@@ -484,35 +492,37 @@
         @pl.when(jnp.logical_not(local))
         def _():
             for i, value in enumerate(values):
-                oo[p, i * part : (i + 1) * part, :] = value
-            out_copy(p).start()
+                oo[p, i * part : (i + 1) * part, span_of(blocks)] = value
+            out_copy(p, blocks).start()
 
     for i in range(2):
         loads["rec", i].wait()
     y_rec[...] = f_rec[1].astype(LOW)
     rec_w[f] = f_rec[0].astype(LOW)
+    pl.semaphore_wait(barrier, len(peers))
+    token_swap.start()
     y_copy(REC).start()
     send_own(REC, 0)
-
-    ext[own] = jnp.broadcast_to(extra[...], ext.shape[1:])
     loads["tok"].wait()
     token_swap.wait()
     norm_rows(tk, gain_one)
     gather_start(0)
+
+    for i in range(2):
+        loads["mix", i].wait()
+    y_mix[...] = (f_mix[1] * mix_scale[...]).astype(LOW)
+    mix_w[f] = (f_mix[0] * mix_scale[...]).astype(LOW)
+    send_own(MIX, 0)
+    send_own(REC, 1)
+    for i in range(extra.shape[0]):
+        lanes = slice(i * block, (i + 1) * block)
+        ext[own, :, lanes] = jnp.broadcast_to(extra[i : i + 1, :], (ext.shape[1], block))
     ext_copies = [
         remote(ext.at[own], ext.at[own], ex_send.at[i], ex_recv.at[i], device)
         for i, device in enumerate((x_dev, y_dev, d_dev))
     ]
     for copy in ext_copies:
         copy.start()
-
-    for i in range(2):
-        loads["mix", i].wait()
-    y_mix[...] = (f_mix[1] * mix_scale[...]).astype(LOW)
-    mix_w[f] = (f_mix[0] * mix_scale[...]).astype(LOW)
-    y_copy(MIX).start()
-    send_own(MIX, 0)
-    send_own(REC, 1)
     for i in range(2):
         for name in ("gate", "up", "down"):
             loads[name, i].wait()
@@ -522,29 +532,45 @@
     y_down[...] = (f_down[1] * down_scale[...]).astype(LOW)
     down_w[f] = (f_down[0] * down_scale[...]).astype(LOW)
 
-    gather_first(0)
     forward(REC, 0, 0)
     forward(REC, 1, 0)
-    send_own(MIX, 1)
+    gather_first(0)
+    y_copy(MIX).start()
+    y_copy(GU).start()
+    y_copy(DOWN).start()
     forward(REC, 0, 1)
     forward(REC, 1, 1)
     gather_second(0)
-    y_copy(GU).start()
-    send_own(GU, 0)
+    forward(MIX, 0, 0)
+    forward(MIX, 1, 0)
     gather_last(0)
     for i, seq in enumerate((own_x, own_y, own_d)):
         remote(ext.at[seq], ext.at[seq], ex_send.at[i], ex_recv.at[i], t_dev).wait_recv()
-    forward(MIX, 0, 0)
-    forward(MIX, 0, 1)
     for p in range(1, 4):
         need(REC, p)
 
     at_chans = pl.multiple_of(q * chans, chans)
 
     def recur(s, carry):
+        @pl.when(s == 1)
+        def _():
+            send_own(MIX, 1)
+            send_own(GU, 0)
+
+        @pl.when(s == 2)
+        def _():
+            forward(MIX, 0, 1)
+
+        @pl.when(s == 3)
+        def _():
+            forward(MIX, 1, 1)
+
         left = nbuf[s].reshape(rows, width)
         total = jnp.dot(left, rec_w[...].reshape(width, chans), preferred_element_type=F32)
-        ri[...] = (total * rec_scale[:, pl.ds(at_chans, chans)]).astype(LOW)
+        for b in range(chans // block):
+            here = slice(b * block, (b + 1) * block)
+            number = q * (chans // block) + b
+            ri[:, here] = (total[:, here] * rec_scale[pl.ds(number, 1), :]).astype(LOW)
         ecol[...] = jnp.broadcast_to(ext[s, 0:1, :], (block, rows)).T
         for b in range(chans // block):
             here = slice(b * block, (b + 1) * block)
@@ -564,7 +590,7 @@
             input_gate = jax.nn.sigmoid(
                 jnp.dot(conv_low, input_blocks[number], preferred_element_type=F32)
             )
-            param = -decay_param[:, lanes]
+            param = -decay_param[pl.ds(number, 1), :]
             soft = jnp.maximum(param, 0.0) + jnp.log1p(jnp.exp(-jnp.abs(param)))
             log_decay = -DECAY_FACTOR * recur_gate * soft + ecol[...]
             decay = jnp.exp(log_decay)
@@ -583,49 +609,50 @@
 
     lax.fori_loop(0, 4, recur, 0)
 
-    forward(MIX, 1, 0)
-    forward(MIX, 1, 1)
-    send_own(GU, 1)
-    y_copy(DOWN).start()
-    send_own(DOWN, 0)
-
     products(0, 0, st, mix_w, MIX)
     products(0, 1, st, mix_w, MIX)
     pair_sums(0, 0)
+    send_own(GU, 1)
+    pair_sums(0, 1)
     products(0, 2, st, mix_w, MIX)
-    pair_sums(0, 1)
     line_sums(0, 0)
-    products(0, 3, st, mix_w, MIX)
     pair_sums(0, 2)
     line_sums(0, 1)
+    products(0, 3, st, mix_w, MIX)
     mix_done(0)
     pair_sums(0, 3)
+    forward(GU, 0, 0)
     line_sums(0, 2)
     mix_done(1)
+    forward(GU, 1, 0)
     line_sums(0, 3)
     mix_done(2)
     mix_done(3)
 
     norm_rows(mx, gain_two)
     gather_start(1)
+    gather_first(1)
+    wait_block(DOWN, fp)
+    forward(GU, 0, 1)
+    gather_second(1)
+    forward(GU, 1, 1)
+    gather_last(1)
+    send_own(DOWN, 0)
     send_own(DOWN, 1)
-    forward(GU, 0, 0)
-    gather_first(1)
-    forward(GU, 1, 0)
-    gather_second(1)
-    forward(GU, 0, 1)
-    gather_last(1)
-    forward(GU, 1, 1)
     for p in range(1, 4):
         need(GU, p)
 
-    at_units = pl.ds(pl.multiple_of(q * units, units), units)
+    unit_rows = units // block
+
+    def unit_scales(scale):
+        first = q * unit_rows
+        return jnp.concatenate([scale[pl.ds(first + i, 1), :] for i in range(unit_rows)], 1)
 
     def hidden(s, carry):
         left = nbuf[s].reshape(rows, width)
         total = jnp.dot(left, gu_w[...].reshape(width, 2 * units), preferred_element_type=F32)
-        gate = total[:, :units] * gate_scale[:, at_units]
-        up = total[:, units:] * up_scale[:, at_units]
+        gate = total[:, :units] * unit_scales(gate_scale)
+        up = total[:, units:] * unit_scales(up_scale)
         value = (gate * jax.nn.sigmoid(gate) * up).astype(LOW)
         hid[s, 0] = value[:half]
         hid[s, 1] = value[half:]
@@ -634,29 +661,40 @@
     lax.fori_loop(0, 4, hidden, 0)
 
     products(1, 0, hid, down_w, DOWN)
+    products(1, 1, hid, down_w, DOWN)
     pair_sums(1, 0)
+    pair_sums(1, 1)
     forward(DOWN, 0, 0)
     forward(DOWN, 0, 1)
     line_sums(1, 0)
+    line_sums(1, 1)
+    down_done(0)
     forward(DOWN, 1, 0)
     forward(DOWN, 1, 1)
-    down_done(0)
-    for p in range(1, 4):
-        products(1, p, hid, down_w, DOWN)
-        pair_sums(1, p)
-        line_sums(1, p)
-        down_done(p)
-
-    for p in range(4):
+    down_done(1)
+    products(1, 2, hid, down_w, DOWN)
+    pair_sums(1, 2)
+    products(1, 3, hid, down_w, DOWN, (0,))
+    line_sums(1, 2)
+    pair_sums(1, 3, (0,))
+    down_done(2)
+    products(1, 3, hid, down_w, DOWN, (1,))
+    line_sums(1, 3, (0,))
+    pair_sums(1, 3, (1,))
+    down_done(3, (0,))
+    line_sums(1, 3, (1,))
+    down_done(3, (1,))
+
+    for p, blocks in ((0, (0, 1)), (1, (0, 1)), (2, (0, 1)), (3, (0,)), (3, (1,))):
         local = lax.div(planes[p], 2) == t
 
         @pl.when(local)
         def _():
-            out_copy(p).wait_recv()
+            out_copy(p, blocks).wait_recv()
 
         @pl.when(jnp.logical_not(local))
         def _():
-            out_copy(p).wait_send()
+            out_copy(p, blocks).wait_send()
 
     result = pltpu.make_async_copy(ob, out, out_sem)
     result.start()
@@ -664,7 +702,7 @@
         y_copy(k).wait_send()
         for j in range(2):
             for i, device in enumerate(near):
-                block_copy(k, f if j == 0 else fp, wo_send.at[k, j, i], device).wait_send()
+                block_copy(k, own_place(k, j), wo_send.at[k, j, i], device).wait_send()
 
         @pl.when(inner)
         def _():
@@ -713,6 +751,9 @@
 
     def row(vector):
         return vector.reshape(1, -1)
+
+    def lines(vector):
+        return vector.reshape(-1, block)
 
     out = pl.pallas_call(
         layer_kernel,
@@ -758,10 +799,10 @@
             dma((2,)),
             dma((3,)),
             dma((3,)),
-            dma((2, 4, 5)),
-            dma((2, 4, 5)),
-            dma((4,)),
-            dma((4,)),
+            dma((2, 4, 10)),
+            dma((2, 4, 10)),
+            dma((4, 2)),
+            dma((4, 2)),
         ],
         compiler_params=pltpu.CompilerParams(
             collective_id=0, has_side_effects=True, vmem_limit_bytes=VMEM_BYTES
@@ -774,16 +815,16 @@
         feedforward_up_weight,
         feedforward_down_weight,
         row(mixing_norm_gain),
-        row(recurrent_input_scale),
+        lines(recurrent_input_scale),
         convolution_kernel_taps,
         recurrence_gate_weight_blocks,
         input_gate_weight_blocks,
-        row(channel_decay_parameter),
-        row(token_extra_log_decay),
+        lines(channel_decay_parameter),
+        lines(token_extra_log_decay),
         row(mixing_output_scale),
         row(feedforward_norm_gain),
-        row(feedforward_gate_scale),
-        row(feedforward_up_scale),
+        lines(feedforward_gate_scale),
+        lines(feedforward_up_scale),
         row(feedforward_down_scale),
     )
     return out.reshape(rows, half_width)

time: 241 us -> 206 us (0.85)
  Pallas kernels: 232 us -> 203 us
  local copies, waits for them, and re-layouts: 8.52 us -> 2.06 us
    pallas_call x1, Pallas kernels: 232 us -> 203 us  [team_body(): pl.pallas_call(layer_kernel, out_shape=jax.ShapeDtypeStruct((2, half, hal...]
    reshape x5 -> x0, local copies, waits for them, and re-layouts: 6.46 us -> none  [row(): return vector.reshape(1, -1)]
where the time goes in v1:
time: 206 us
  Pallas kernels  203 us (99%)
  local copies, waits for them, and re-layouts  2.06 us (1%)
    pallas_call x1, Pallas kernels, team_body(): pl.pallas_call(layer_kernel, out_shape=jax.ShapeDtypeStruct((2, half, hal...  203 us

profile of v1, /device:TPU:0, one launch (start us, length us, event | category | flops | bytes accessed | tf_op | source)
XLA Modules:
  0.0 205.5 jit_solution(14129731225517653239)
XLA Ops:
  0.0 203.5 %shard_map.172 = bf16[2,192,1024]{2,1,0:T(8,128)(2,1)} custom-call(bf16[384,1024]{1,0:T(8,128)(2,1)} %tokens.1, f32[256,1536]{1,0:T(8,128)} %w_rec.1, f32[1536,256]{1,0:T(8,128)} %w_mix.1, f32[256,2560]{1,0:T(8,128)} %w_gate.1, f32[256,2560]{1,0:T(8,128)} %w_up.1, f32[2560,256]{1,0:T(8,128)} %w_down.1, f32[1,2048]{1,0:T(1,128)} %bitcast.13, ...), custom_call_target="tpu_custom_call" | custom-call | tf_op jit(solution)/shard_map/pallas_call | solution.py:758
  203.5 2.1 %copy.20 = bf16[384,1024]{1,0:T(8,128)(2,1)} copy(bf16[384,1024]{1,0:T(8,128)(2,1)} %bitcast.10) | data formatting | bytes 1572864

commit v2 on v1

--- a/solution.py
+++ b/solution.py
@@ -142,6 +142,7 @@
 
 
 REC, MIX, GU, DOWN = range(4)
+PIECE_PLACE = {0: 0, 2: 1, 3: 2}
 LOW = jnp.bfloat16
 F32 = jnp.float32
 
@@ -167,8 +168,8 @@
     gain_one,
     rec_scale,
     taps,
-    recur_blocks,
-    input_blocks,
+    w_recur,
+    w_input,
     decay_param,
     extra,
     mix_scale,
@@ -203,9 +204,11 @@
     r1,
     r2,
     oo,
-    ob,
+    recur_blocks,
+    input_blocks,
     load_sem,
-    out_sem,
+    wl_send,
+    wl_recv,
     wy_send,
     wo_send,
     wf_send,
@@ -226,6 +229,7 @@
     chans = rec_w.shape[2]
     units = down_w.shape[1]
     cols = mix_w.shape[2]
+    unit = cols // 2
     block = recur_blocks.shape[1]
     tap_count = taps.shape[0]
 
@@ -266,6 +270,9 @@
         load(("gate", i), 5 + i, w_gate.at[:, at], f_gu.at[i, 0])
         load(("up", i), 7 + i, w_up.at[:, at], f_gu.at[i, 1])
         load(("down", i), 9 + i, w_down.at[at, :], f_down.at[i])
+    gate_blocks = pl.ds(q * (chans // block), chans // block)
+    load("recur", 11, w_recur.at[gate_blocks], recur_blocks)
+    load("input", 12, w_input.at[gate_blocks], input_blocks)
 
     barrier = pltpu.get_barrier_semaphore()
     peers = [x_dev, y_dev, t_dev, d_dev]
@@ -288,8 +295,11 @@
     def send_own(k, j):
         if j == 1 and k != DOWN:
             wait_block(k, fp)
-        for i, device in enumerate(near):
-            block_copy(k, own_place(k, j), wo_send.at[k, j, i], device).start()
+        for i in range(2):
+            send_one(k, j, i)
+
+    def send_one(k, j, i):
+        block_copy(k, own_place(k, j), wo_send.at[k, j, i], near[i]).start()
 
     y_bufs = (y_rec, y_mix, y_gu, y_down)
 
@@ -302,17 +312,42 @@
         edge = 3 * (z - 1)
         return place, block_copy(k, place, wf_send.at[k, far, j], {"fs": edge * 2 + y})
 
+    def forward_copies(k, far, j):
+        place, copy = forward_copy(k, far, j)
+        if k == DOWN and far and j:
+            return place, last_copies(place, {"fs": 3 * (z - 1) * 2 + y})
+        return place, [copy]
+
     def forward(k, far, j):
         @pl.when(inner)
         def _():
-            place, copy = forward_copy(k, far, j)
+            place, copies = forward_copies(k, far, j)
             wait_block(k, place)
-            copy.start()
-
-    def need(k, p, blocks=(0, 1)):
+            for copy in copies:
+                copy.start()
+
+    def last_copies(place, device):
+        view = down_w.at[place]
+        return [
+            remote(
+                view.at[:, pl.ds(i * unit, unit)],
+                view.at[:, pl.ds(i * unit, unit)],
+                wl_send.at[i],
+                wl_recv.at[i],
+                device,
+            )
+            for i in range(2)
+        ]
+
+    def need(k, p, piece=(0, 4)):
         def wait():
-            for j in blocks:
-                wait_block(k, planes[p] * 2 + j)
+            for j in range(2):
+                if k == DOWN and p == 3 and j == 1:
+                    for i, copy in enumerate(last_copies(planes[p] * 2 + j, y_dev)):
+                        if piece[0] <= 2 + i < sum(piece):
+                            copy.wait_recv()
+                elif piece[0] <= 2 * j < sum(piece):
+                    wait_block(k, planes[p] * 2 + j)
 
         if p == 1:
             wait()
@@ -346,7 +381,7 @@
             (own_d, low, t_dev),
         )[role]
         view = nbuf.at[seq, t, at, :]
-        return remote(view, view, g_send.at[phase, role], g_recv.at[phase, role], device)
+        return remote(view, view, g_send.at[role], g_recv.at[role], device)
 
     def rows_wait(phase, role):
         seq, side_at, at = (
@@ -365,7 +400,7 @@
             (own_d, 1 - t, low),
         )[role]
         view = nbuf.at[seq, side_at, at, :]
-        remote(view, view, g_send.at[phase, role], g_recv.at[phase, role], t_dev).wait_recv()
+        remote(view, view, g_send.at[role], g_recv.at[role], t_dev).wait_recv()
 
     def gather_start(phase):
         for role in (1, 2, 0, 3, 6):
@@ -395,27 +430,30 @@
         for role in range(13):
             rows_copy(phase, role).wait_send()
 
-    def products(phase, p, left, weights, k, blocks=(0, 1)):
-        need(k, p, blocks)
-        first = planes[p] * 2
-
-        def product(side, c):
+    def products(phase, p, left, weights, k, piece=(0, 4)):
+        need(k, p, piece)
+        first, size = planes[p] * 2, min(piece[1], 2)
+
+        def product(side, start):
             rows_now = left[:, side].reshape(4 * half, left.shape[-1])
-            value = jnp.dot(rows_now, weights[first + c], preferred_element_type=F32)
-            return value.astype(LOW).reshape(4, half, cols)
-
-        for c in blocks:
-            oth[p, :, :, c * cols : (c + 1) * cols] = product(1 - t, c)
-        sum_copies(phase, p, 0, blocks).start()
-        for c in blocks:
-            value = product(t, c).reshape(2, 2, half, cols)
-            kept[p, :, :, :, c * cols : (c + 1) * cols] = value
-
-    def span_of(blocks):
-        return pl.ds(blocks[0] * cols, len(blocks) * cols)
-
-    def sum_copies(phase, p, number, blocks):
-        at = span_of(blocks)
+            column = start % 2 * unit
+            weight = weights[first + start // 2, :, column : column + size * unit]
+            value = jnp.dot(rows_now, weight, preferred_element_type=F32)
+            return value.astype(LOW).reshape(4, half, size * unit)
+
+        starts = range(piece[0], sum(piece), size)
+        for start in starts:
+            oth[p, :, :, start * unit : (start + size) * unit] = product(1 - t, start)
+        sum_copies(phase, p, 0, piece).start()
+        for start in starts:
+            value = product(t, start).reshape(2, 2, half, size * unit)
+            kept[p, :, :, :, start * unit : (start + size) * unit] = value
+
+    def span_of(piece):
+        return pl.ds(piece[0] * unit, piece[1] * unit)
+
+    def sum_copies(phase, p, number, piece):
+        at = span_of(piece)
         src, dst, device = (
             (oth.at[p, :, :, at], rt.at[phase, p, :, :, at], t_dev),
             (kept.at[p, 1 - r, :, top, at], r1.at[phase, p, 0, :, :, at], x_dev),
@@ -423,12 +461,12 @@
             (kept.at[p, r, 1 - y, top, at], r2.at[phase, p, 0, :, at], y_dev),
             (kept.at[p, 1 - r, y, low, at], r2.at[phase, p, 1, :, at], x_dev),
         )[number]
-        number += 5 * blocks[0]
-        return remote(src, dst, m_send.at[phase, p, number], m_recv.at[phase, p, number], device)
-
-    def pair_sums(phase, p, blocks=(0, 1)):
-        sum_copies(phase, p, 0, blocks).wait_recv()
-        at = span_of(blocks)
+        send, land = p + PIECE_PLACE[piece[0]], p + PIECE_PLACE[piece[0]] + 4 * phase
+        return remote(src, dst, m_send.at[send, number], m_recv.at[land, number], device)
+
+    def pair_sums(phase, p, piece=(0, 4)):
+        sum_copies(phase, p, 0, piece).wait_recv()
+        at = span_of(piece)
 
         def step(s, carry):
             a, b = lax.div(s, 2), lax.rem(s, 2)
@@ -437,63 +475,63 @@
             return carry
 
         lax.fori_loop(0, 4, step, 0)
-        sum_copies(phase, p, 1, blocks).start()
-        sum_copies(phase, p, 2, blocks).start()
-
-    def line_sums(phase, p, blocks=(0, 1)):
-        at = span_of(blocks)
-        sum_copies(phase, p, 1, blocks).wait_recv()
+        sum_copies(phase, p, 1, piece).start()
+        sum_copies(phase, p, 2, piece).start()
+
+    def line_sums(phase, p, piece=(0, 4)):
+        at = span_of(piece)
+        sum_copies(phase, p, 1, piece).wait_recv()
         for i in range(2):
             value = kept[p, r, i, top, at].astype(F32) + r1[phase, p, 0, i, :, at].astype(F32)
             kept[p, r, i, top, at] = value.astype(LOW)
-        sum_copies(phase, p, 3, blocks).start()
-        sum_copies(phase, p, 2, blocks).wait_recv()
+        sum_copies(phase, p, 3, piece).start()
+        sum_copies(phase, p, 2, piece).wait_recv()
         for i in range(2):
             value = kept[p, i, y, low, at].astype(F32) + r1[phase, p, 1, i, :, at].astype(F32)
             kept[p, i, y, low, at] = value.astype(LOW)
-        sum_copies(phase, p, 4, blocks).start()
-
-    def columns_of(plane, blocks):
-        start = pl.multiple_of((plane * 2 + blocks[0]) * cols, cols)
-        return pl.ds(start, len(blocks) * cols)
-
-    def last_sums(phase, p, base, blocks):
-        at, piece = columns_of(planes[p], blocks), span_of(blocks)
+        sum_copies(phase, p, 4, piece).start()
+
+    def columns_of(plane, piece):
+        start = pl.multiple_of((plane * 4 + piece[0]) * unit, unit)
+        return pl.ds(start, piece[1] * unit)
+
+    def last_sums(phase, p, base, piece):
+        at, inside = columns_of(planes[p], piece), span_of(piece)
         values = []
         for i, number in enumerate((3, 4)):
             span = slice(i * part, (i + 1) * part)
-            sum_copies(phase, p, number, blocks).wait_recv()
-            value = kept[p, r, y, span, piece].astype(F32) + r2[phase, p, i, :, piece].astype(F32)
+            sum_copies(phase, p, number, piece).wait_recv()
+            value = kept[p, r, y, span, inside].astype(F32) + r2[phase, p, i, :, inside].astype(F32)
             values.append((base[span, at].astype(F32) + value).astype(LOW))
         for number in range(5):
-            sum_copies(phase, p, number, blocks).wait_send()
+            sum_copies(phase, p, number, piece).wait_send()
         return at, values
 
     def mix_done(p):
-        at, values = last_sums(0, p, tk, (0, 1))
+        at, values = last_sums(0, p, tk, (0, 4))
         for i, value in enumerate(values):
             mx[i * part : (i + 1) * part, at] = value
 
-    def out_copy(p, blocks):
-        at = columns_of(lax.rem(planes[p], 2), blocks)
-        src = oo.at[p, :, span_of(blocks)]
-        return remote(src, ob.at[t, :, at], o_send.at[p, blocks[0]], o_recv.at[p, blocks[0]], t_dev)
-
-    def down_done(p, blocks=(0, 1)):
-        _, values = last_sums(1, p, mx, blocks)
+    def out_copy(p, piece):
+        at = columns_of(lax.rem(planes[p], 2), piece)
+        src = oo.at[p, :, span_of(piece)]
+        return remote(src, out.at[t, :, at], o_send.at[p + PIECE_PLACE[piece[0]]], o_recv.at[p + PIECE_PLACE[piece[0]]], t_dev)
+
+    def down_done(p, piece=(0, 4)):
+        _, values = last_sums(1, p, mx, piece)
         local = lax.div(planes[p], 2) == t
-        at = columns_of(lax.rem(planes[p], 2), blocks)
+        at = columns_of(lax.rem(planes[p], 2), piece)
 
         @pl.when(local)
         def _():
             for i, value in enumerate(values):
-                ob[t, i * part : (i + 1) * part, at] = value
+                out[t, i * part : (i + 1) * part, at] = value
 
         @pl.when(jnp.logical_not(local))
         def _():
             for i, value in enumerate(values):
-                oo[p, i * part : (i + 1) * part, span_of(blocks)] = value
-            out_copy(p, blocks).start()
+                oo[p, i * part : (i + 1) * part, span_of(piece)] = value
+            out_copy(p, piece).start()
 
     for i in range(2):
         loads["rec", i].wait()
@@ -512,7 +550,12 @@
         loads["mix", i].wait()
     y_mix[...] = (f_mix[1] * mix_scale[...]).astype(LOW)
     mix_w[f] = (f_mix[0] * mix_scale[...]).astype(LOW)
-    send_own(MIX, 0)
+
+
+    @pl.when(inner)
+    def _():
+        send_one(MIX, 0, 1)
+
     send_own(REC, 1)
     for i in range(extra.shape[0]):
         lanes = slice(i * block, (i + 1) * block)
@@ -532,6 +575,12 @@
     y_down[...] = (f_down[1] * down_scale[...]).astype(LOW)
     down_w[f] = (f_down[0] * down_scale[...]).astype(LOW)
 
+    send_one(MIX, 0, 0)
+
+    @pl.when(jnp.logical_not(inner))
+    def _():
+        send_one(MIX, 0, 1)
+
     forward(REC, 0, 0)
     forward(REC, 1, 0)
     gather_first(0)
@@ -548,6 +597,8 @@
         remote(ext.at[seq], ext.at[seq], ex_send.at[i], ex_recv.at[i], t_dev).wait_recv()
     for p in range(1, 4):
         need(REC, p)
+    loads["recur"].wait()
+    loads["input"].wait()
 
     at_chans = pl.multiple_of(q * chans, chans)
 
@@ -585,10 +636,10 @@
                 conv_out = conv_out + taps[tap : tap + 1, lanes] * moved
             conv_low = conv_out.astype(LOW)
             recur_gate = jax.nn.sigmoid(
-                jnp.dot(conv_low, recur_blocks[number], preferred_element_type=F32)
+                jnp.dot(conv_low, recur_blocks[b], preferred_element_type=F32)
             )
             input_gate = jax.nn.sigmoid(
-                jnp.dot(conv_low, input_blocks[number], preferred_element_type=F32)
+                jnp.dot(conv_low, input_blocks[b], preferred_element_type=F32)
             )
             param = -decay_param[pl.ds(number, 1), :]
             soft = jnp.maximum(param, 0.0) + jnp.log1p(jnp.exp(-jnp.abs(param)))
@@ -660,44 +711,47 @@
 
     lax.fori_loop(0, 4, hidden, 0)
 
+    last_pieces = ((0, 2), (2, 1), (3, 1))
     products(1, 0, hid, down_w, DOWN)
+    pair_sums(1, 0)
     products(1, 1, hid, down_w, DOWN)
-    pair_sums(1, 0)
+    forward(DOWN, 0, 0)
+    line_sums(1, 0)
     pair_sums(1, 1)
-    forward(DOWN, 0, 0)
     forward(DOWN, 0, 1)
-    line_sums(1, 0)
-    line_sums(1, 1)
     down_done(0)
     forward(DOWN, 1, 0)
+    line_sums(1, 1)
     forward(DOWN, 1, 1)
     down_done(1)
     products(1, 2, hid, down_w, DOWN)
     pair_sums(1, 2)
-    products(1, 3, hid, down_w, DOWN, (0,))
+    products(1, 3, hid, down_w, DOWN, last_pieces[0])
     line_sums(1, 2)
-    pair_sums(1, 3, (0,))
+    pair_sums(1, 3, last_pieces[0])
+    products(1, 3, hid, down_w, DOWN, last_pieces[1])
     down_done(2)
-    products(1, 3, hid, down_w, DOWN, (1,))
-    line_sums(1, 3, (0,))
-    pair_sums(1, 3, (1,))
-    down_done(3, (0,))
-    line_sums(1, 3, (1,))
-    down_done(3, (1,))
-
-    for p, blocks in ((0, (0, 1)), (1, (0, 1)), (2, (0, 1)), (3, (0,)), (3, (1,))):
+    pair_sums(1, 3, last_pieces[1])
+    line_sums(1, 3, last_pieces[0])
+    products(1, 3, hid, down_w, DOWN, last_pieces[2])
+    pair_sums(1, 3, last_pieces[2])
+    line_sums(1, 3, last_pieces[1])
+    down_done(3, last_pieces[0])
+    line_sums(1, 3, last_pieces[2])
+    down_done(3, last_pieces[1])
+    down_done(3, last_pieces[2])
+
+    for p, piece in ((0, (0, 4)), (1, (0, 4)), (2, (0, 4)), (3, (0, 2)), (3, (2, 1)), (3, (3, 1))):
         local = lax.div(planes[p], 2) == t
 
         @pl.when(local)
         def _():
-            out_copy(p, blocks).wait_recv()
+            out_copy(p, piece).wait_recv()
 
         @pl.when(jnp.logical_not(local))
         def _():
-            out_copy(p, blocks).wait_send()
-
-    result = pltpu.make_async_copy(ob, out, out_sem)
-    result.start()
+            out_copy(p, piece).wait_send()
+
     for k in range(4):
         y_copy(k).wait_send()
         for j in range(2):
@@ -708,11 +762,11 @@
         def _():
             for far in range(2):
                 for j in range(2):
-                    forward_copy(k, far, j)[1].wait_send()
+                    for copy in forward_copies(k, far, j)[1]:
+                        copy.wait_send()
 
     for copy in ext_copies:
         copy.wait_send()
-    result.wait()
 
 
 def team_body(
@@ -757,9 +811,9 @@
 
     out = pl.pallas_call(
         layer_kernel,
-        out_shape=jax.ShapeDtypeStruct((2, half, half_width), LOW),
-        in_specs=[any_spec] * 6 + [vmem_spec] * 12,
-        out_specs=any_spec,
+        out_shape=vmem((2, half, half_width), LOW),
+        in_specs=[any_spec] * 6 + [vmem_spec] * 3 + [any_spec] * 2 + [vmem_spec] * 7,
+        out_specs=vmem_spec,
         scratch_shapes=[
             vmem((4, 2, half, width), LOW),
             vmem((planes, depth, chans), LOW),
@@ -787,22 +841,24 @@
             vmem((2, 4, 2, 2, part, 2 * cols), LOW),
             vmem((2, 4, 2, part, 2 * cols), LOW),
             vmem((4, half, 2 * cols), LOW),
-            vmem((2, half, half_width), LOW),
-            dma((11,)),
-            dma,
+            vmem((chans // block, block, block), LOW),
+            vmem((chans // block, block, block), LOW),
+            dma((13,)),
+            dma((2,)),
+            dma((2,)),
             dma((4,)),
             dma((4, 2, 2)),
             dma((4, 2, 2)),
             dma((4, planes)),
-            dma((2, 13)),
-            dma((2, 13)),
+            dma((13,)),
+            dma((13,)),
             dma((2,)),
             dma((3,)),
             dma((3,)),
-            dma((2, 4, 10)),
-            dma((2, 4, 10)),
-            dma((4, 2)),
-            dma((4, 2)),
+            dma((6, 5)),
+            dma((10, 5)),
+            dma((6,)),
+            dma((6,)),
         ],
         compiler_params=pltpu.CompilerParams(
             collective_id=0, has_side_effects=True, vmem_limit_bytes=VMEM_BYTES
@@ -830,7 +886,7 @@
     return out.reshape(rows, half_width)
 
 
-VMEM_BYTES = 66_000_000
+VMEM_BYTES = 60_000_000
 
 
 def team_fits(mesh):
@@ -862,7 +918,7 @@
 
     def body(*args):
         blocks, hidden, rows = args[5].shape[0], args[12].shape[1], args[0].shape[0]
-        if not team_fits(mesh) or blocks % 4 or hidden % 512 or rows % 64:
+        if not team_fits(mesh) or blocks % 4 or hidden % 512 or rows % 64 or args[9].shape[1] % 256:
             return plain_body(*args)
         return team_body(*args)
 

time: 206 us -> 200 us (0.971)
  Pallas kernels: 203 us -> 199 us
    pallas_call x1, Pallas kernels: 203 us -> 199 us  [team_body(): pl.pallas_call(layer_kernel, out_shape=vmem((2, half, half_width), LOW),...]
where the time goes in v2:
time: 200 us
  Pallas kernels  199 us (100%)
    pallas_call x1, Pallas kernels, team_body(): pl.pallas_call(layer_kernel, out_shape=vmem((2, half, half_width), LOW),...  199 us

profile of v2, /device:TPU:0, one launch (start us, length us, event | category | flops | bytes accessed | tf_op | source)
XLA Modules:
  0.0 200.0 jit_solution(13322860342672747495)
XLA Ops:
  0.0 199.2 %shard_map.172 = bf16[2,192,1024]{2,1,0:T(8,128)(2,1)S(1)} custom-call(bf16[384,1024]{1,0:T(8,128)(2,1)} %tokens.1, f32[256,1536]{1,0:T(8,128)} %w_rec.1, f32[1536,256]{1,0:T(8,128)} %w_mix.1, f32[256,2560]{1,0:T(8,128)} %w_gate.1, f32[256,2560]{1,0:T(8,128)} %w_up.1, f32[2560,256]{1,0:T(8,128)} %w_down.1, f32[1,2048]{1,0:T(1,128)} %bitcast.13, ...), custom_call_target="tpu_custom_call" | custom-call | tf_op jit(solution)/shard_map/pallas_call | solution.py:812
  199.2 0.9 copy.20

commit v3 on v2

--- a/solution.py
+++ b/solution.py
@@ -142,7 +142,7 @@
 
 
 REC, MIX, GU, DOWN = range(4)
-PIECE_PLACE = {0: 0, 2: 1, 3: 2}
+PIECES = ((0, 0), (1, 0), (2, 0), (2, 2), (3, 0), (3, 2), (3, 3))
 LOW = jnp.bfloat16
 F32 = jnp.float32
 
@@ -203,6 +203,7 @@
     rt,
     r1,
     r2,
+    rd,
     oo,
     recur_blocks,
     input_blocks,
@@ -461,8 +462,17 @@
             (kept.at[p, r, 1 - y, top, at], r2.at[phase, p, 0, :, at], y_dev),
             (kept.at[p, 1 - r, y, low, at], r2.at[phase, p, 1, :, at], x_dev),
         )[number]
-        send, land = p + PIECE_PLACE[piece[0]], p + PIECE_PLACE[piece[0]] + 4 * phase
-        return remote(src, dst, m_send.at[send, number], m_recv.at[land, number], device)
+        return remote(src, dst, *sum_sems(phase, p, number, piece), device)
+
+    def sum_sems(phase, p, number, piece):
+        place = PIECES.index((p, piece[0])) if phase else p
+        return m_send.at[place, number], m_recv.at[4 * phase + place, number]
+
+    def direct_copy(p, number, piece):
+        at, device = span_of(piece), (x_dev, y_dev, d_dev)[number]
+        a, b = ((1 - r, y), (r, 1 - y), (1 - r, 1 - y))[number]
+        src, dst = kept.at[p, a, b, :, at], rd.at[piece[0] % 2, number]
+        return remote(src, dst, *sum_sems(1, p, 1 + number, piece), device)
 
     def pair_sums(phase, p, piece=(0, 4)):
         sum_copies(phase, p, 0, piece).wait_recv()
@@ -475,8 +485,12 @@
             return carry
 
         lax.fori_loop(0, 4, step, 0)
-        sum_copies(phase, p, 1, piece).start()
-        sum_copies(phase, p, 2, piece).start()
+        if piece[1] == 1:
+            for number in (2, 0, 1):
+                direct_copy(p, number, piece).start()
+        else:
+            sum_copies(phase, p, 1, piece).start()
+            sum_copies(phase, p, 2, piece).start()
 
     def line_sums(phase, p, piece=(0, 4)):
         at = span_of(piece)
@@ -497,6 +511,16 @@
 
     def last_sums(phase, p, base, piece):
         at, inside = columns_of(planes[p], piece), span_of(piece)
+        if piece[1] == 1:
+            total = kept[p, r, y, :, inside].astype(F32)
+            for number in range(3):
+                direct_copy(p, number, piece).wait_recv()
+                total = total + rd[piece[0] % 2, number].astype(F32)
+            value = (base[:, at].astype(F32) + total).astype(LOW)
+            sum_copies(phase, p, 0, piece).wait_send()
+            for number in range(3):
+                direct_copy(p, number, piece).wait_send()
+            return at, [value[:part], value[part:]]
         values = []
         for i, number in enumerate((3, 4)):
             span = slice(i * part, (i + 1) * part)
@@ -514,8 +538,8 @@
 
     def out_copy(p, piece):
         at = columns_of(lax.rem(planes[p], 2), piece)
-        src = oo.at[p, :, span_of(piece)]
-        return remote(src, out.at[t, :, at], o_send.at[p + PIECE_PLACE[piece[0]]], o_recv.at[p + PIECE_PLACE[piece[0]]], t_dev)
+        src, place = oo.at[p, :, span_of(piece)], PIECES.index((p, piece[0]))
+        return remote(src, out.at[t, :, at], o_send.at[place], o_recv.at[place], t_dev)
 
     def down_done(p, piece=(0, 4)):
         _, values = last_sums(1, p, mx, piece)
@@ -711,37 +735,43 @@
 
     lax.fori_loop(0, 4, hidden, 0)
 
-    last_pieces = ((0, 2), (2, 1), (3, 1))
-    products(1, 0, hid, down_w, DOWN)
+    first, second, third, fourth = (0, 2), (2, 2), (2, 1), (3, 1)
+
+    def down_products(p, piece=(0, 4)):
+        products(1, p, hid, down_w, DOWN, piece)
+
+    down_products(0)
     pair_sums(1, 0)
-    products(1, 1, hid, down_w, DOWN)
+    down_products(1)
     forward(DOWN, 0, 0)
+    pair_sums(1, 1)
     line_sums(1, 0)
-    pair_sums(1, 1)
     forward(DOWN, 0, 1)
+    forward(DOWN, 1, 0)
+    down_products(2, first)
+    pair_sums(1, 2, first)
     down_done(0)
-    forward(DOWN, 1, 0)
     line_sums(1, 1)
+    line_sums(1, 2, first)
     forward(DOWN, 1, 1)
+    down_products(2, second)
+    pair_sums(1, 2, second)
     down_done(1)
-    products(1, 2, hid, down_w, DOWN)
-    pair_sums(1, 2)
-    products(1, 3, hid, down_w, DOWN, last_pieces[0])
-    line_sums(1, 2)
-    pair_sums(1, 3, last_pieces[0])
-    products(1, 3, hid, down_w, DOWN, last_pieces[1])
-    down_done(2)
-    pair_sums(1, 3, last_pieces[1])
-    line_sums(1, 3, last_pieces[0])
-    products(1, 3, hid, down_w, DOWN, last_pieces[2])
-    pair_sums(1, 3, last_pieces[2])
-    line_sums(1, 3, last_pieces[1])
-    down_done(3, last_pieces[0])
-    line_sums(1, 3, last_pieces[2])
-    down_done(3, last_pieces[1])
-    down_done(3, last_pieces[2])
-
-    for p, piece in ((0, (0, 4)), (1, (0, 4)), (2, (0, 4)), (3, (0, 2)), (3, (2, 1)), (3, (3, 1))):
+    down_done(2, first)
+    line_sums(1, 2, second)
+    down_products(3, first)
+    pair_sums(1, 3, first)
+    down_products(3, third)
+    down_done(2, second)
+    pair_sums(1, 3, third)
+    line_sums(1, 3, first)
+    down_products(3, fourth)
+    pair_sums(1, 3, fourth)
+    down_done(3, first)
+    down_done(3, third)
+    down_done(3, fourth)
+
+    for p, piece in ((0, (0, 4)), (1, (0, 4)), (2, first), (2, second), (3, first), (3, third), (3, fourth)):
         local = lax.div(planes[p], 2) == t
 
         @pl.when(local)
@@ -840,6 +870,7 @@
             vmem((2, 4, 4, half, 2 * cols), LOW),
             vmem((2, 4, 2, 2, part, 2 * cols), LOW),
             vmem((2, 4, 2, part, 2 * cols), LOW),
+            vmem((2, 3, half, cols // 2), LOW),
             vmem((4, half, 2 * cols), LOW),
             vmem((chans // block, block, block), LOW),
             vmem((chans // block, block, block), LOW),
@@ -855,10 +886,10 @@
             dma((2,)),
             dma((3,)),
             dma((3,)),
-            dma((6, 5)),
-            dma((10, 5)),
-            dma((6,)),
-            dma((6,)),
+            dma((len(PIECES), 5)),
+            dma((4 + len(PIECES), 5)),
+            dma((len(PIECES),)),
+            dma((len(PIECES),)),
         ],
         compiler_params=pltpu.CompilerParams(
             collective_id=0, has_side_effects=True, vmem_limit_bytes=VMEM_BYTES

time: 200 us -> 194 us (0.970)
  Pallas kernels: 199 us -> 193 us
    pallas_call x1, Pallas kernels: 199 us -> 193 us  [team_body(): pl.pallas_call(layer_kernel, out_shape=vmem((2, half, half_width), LOW),...]
where the time goes in v3:
time: 194 us
  Pallas kernels  193 us (99%)
    pallas_call x1, Pallas kernels, team_body(): pl.pallas_call(layer_kernel, out_shape=vmem((2, half, half_width), LOW),...  193 us

profile of v3, /device:TPU:0, one launch (start us, length us, event | category | flops | bytes accessed | tf_op | source)
XLA Modules:
  0.0 194.3 jit_solution(8624457263629422827)
XLA Ops:
  0.0 193.4 %shard_map.172 = bf16[2,192,1024]{2,1,0:T(8,128)(2,1)S(1)} custom-call(bf16[384,1024]{1,0:T(8,128)(2,1)} %tokens.1, f32[256,1536]{1,0:T(8,128)} %w_rec.1, f32[1536,256]{1,0:T(8,128)} %w_mix.1, f32[256,2560]{1,0:T(8,128)} %w_gate.1, f32[256,2560]{1,0:T(8,128)} %w_up.1, f32[2560,256]{1,0:T(8,128)} %w_down.1, f32[1,2048]{1,0:T(1,128)} %bitcast.13, ...), custom_call_target="tpu_custom_call" | custom-call | tf_op jit(solution)/shard_map/pallas_call | solution.py:842
  193.4 0.9 copy.20

commit v4 on v3

--- a/solution.py
+++ b/solution.py
@@ -208,7 +208,6 @@
     recur_blocks,
     input_blocks,
     load_sem,
-    wl_send,
     wl_recv,
     wy_send,
     wo_send,
@@ -217,12 +216,10 @@
     g_send,
     g_recv,
     tt_sem,
-    ex_send,
-    ex_recv,
+    ex_sem,
     m_send,
     m_recv,
-    o_send,
-    o_recv,
+    o_sem,
 ):
     rows, half_width = tokens.shape
     half, part = rows // 2, rows // 4
@@ -248,38 +245,45 @@
     mats = (rec_w, mix_w, gu_w, down_w)
     top, low = pl.ds(0, part), pl.ds(part, part)
 
+    barrier = pltpu.get_barrier_semaphore()
+
+    def greet(device):
+        pl.semaphore_signal(barrier, inc=1, device_id=device, device_id_type=pl.DeviceIdType.MESH)
+
+    for device in (x_dev, y_dev, t_dev, d_dev, near[0]):
+        greet(device)
+
+    @pl.when(inner)
+    def _():
+        greet({"fs": y})
+        greet({"fs": 6 + y})
+
     quarters = (q, r * 2 + 1 - y)
-    loads = {}
-
-    def load(name, number, src, dst):
-        copy = pltpu.make_async_copy(src, dst, load_sem.at[number])
-        copy.start()
-        loads[name] = copy
+
+    def load(number, src, dst):
+        pltpu.make_async_copy(src, dst, load_sem.at[number]).start()
+
+    def loaded(number, whole):
+        pltpu.make_async_copy(whole, whole, load_sem.at[number]).wait()
 
     mine = pl.ds(pl.multiple_of(t * half, half), half)
     theirs = pl.ds(pl.multiple_of((1 - t) * half, half), half)
     side = pl.ds(pl.multiple_of(t * half_width, half_width), half_width)
-    load("tok", 0, tokens.at[mine, :], tk.at[:, side])
     for i, piece in enumerate(quarters):
         at = pl.ds(pl.multiple_of(piece * chans, chans), chans)
-        load(("rec", i), 1 + i, w_rec.at[:, at], f_rec.at[i])
+        load(REC, w_rec.at[:, at], f_rec.at[i])
+    load(4, tokens.at[mine, :], tk.at[:, side])
     for i, piece in enumerate(quarters):
         at = pl.ds(pl.multiple_of(piece * chans, chans), chans)
-        load(("mix", i), 3 + i, w_mix.at[at, :], f_mix.at[i])
+        load(MIX, w_mix.at[at, :], f_mix.at[i])
     for i, piece in enumerate(quarters):
         at = pl.ds(pl.multiple_of(piece * units, units), units)
-        load(("gate", i), 5 + i, w_gate.at[:, at], f_gu.at[i, 0])
-        load(("up", i), 7 + i, w_up.at[:, at], f_gu.at[i, 1])
-        load(("down", i), 9 + i, w_down.at[at, :], f_down.at[i])
+        load(GU, w_gate.at[:, at], f_gu.at[i, 0])
+        load(GU, w_up.at[:, at], f_gu.at[i, 1])
+        load(DOWN, w_down.at[at, :], f_down.at[i])
     gate_blocks = pl.ds(q * (chans // block), chans // block)
-    load("recur", 11, w_recur.at[gate_blocks], recur_blocks)
-    load("input", 12, w_input.at[gate_blocks], input_blocks)
-
-    barrier = pltpu.get_barrier_semaphore()
-    peers = [x_dev, y_dev, t_dev, d_dev]
-    peers += [{"fs": plane * 2 + y} for plane in planes[1:]]
-    for device in peers:
-        pl.semaphore_signal(barrier, inc=1, device_id=device, device_id_type=pl.DeviceIdType.MESH)
+    load(5, w_recur.at[gate_blocks], recur_blocks)
+    load(6, w_input.at[gate_blocks], input_blocks)
 
     token_swap = remote(tokens.at[theirs, :], tk.at[:, side], tt_sem.at[0], tt_sem.at[1], t_dev)
 
@@ -288,7 +292,7 @@
         return remote(view, view, send_sem, w_recv.at[k, place], device)
 
     def wait_block(k, place):
-        block_copy(k, place, wo_send.at[0, 0, 0], y_dev).wait_recv()
+        block_copy(k, place, wo_send.at[0], y_dev).wait_recv()
 
     def own_place(k, j):
         return z * 2 + j if k == DOWN else (f if j == 0 else fp)
@@ -300,7 +304,10 @@
             send_one(k, j, i)
 
     def send_one(k, j, i):
-        block_copy(k, own_place(k, j), wo_send.at[k, j, i], near[i]).start()
+        block_copy(k, own_place(k, j), wo_send.at[k], near[i]).start()
+
+    def sent(view, sem):
+        remote(view, view, sem, w_recv.at[0, 0], y_dev).wait_send()
 
     y_bufs = (y_rec, y_mix, y_gu, y_down)
 
@@ -311,7 +318,7 @@
         plane = 3 * (2 - z) if far else 3 - z
         place = plane * 2 + (j if k == DOWN else (y if j == 0 else 1 - y))
         edge = 3 * (z - 1)
-        return place, block_copy(k, place, wf_send.at[k, far, j], {"fs": edge * 2 + y})
+        return place, block_copy(k, place, wf_send.at[k], {"fs": edge * 2 + y})
 
     def forward_copies(k, far, j):
         place, copy = forward_copy(k, far, j)
@@ -333,7 +340,7 @@
             remote(
                 view.at[:, pl.ds(i * unit, unit)],
                 view.at[:, pl.ds(i * unit, unit)],
-                wl_send.at[i],
+                wf_send.at[DOWN],
                 wl_recv.at[i],
                 device,
             )
@@ -382,26 +389,22 @@
             (own_d, low, t_dev),
         )[role]
         view = nbuf.at[seq, t, at, :]
-        return remote(view, view, g_send.at[role], g_recv.at[role], device)
+        return remote(view, view, g_send.at[role // 7], g_recv.at[min(role, 6)], device)
 
     def rows_wait(phase, role):
-        seq, side_at, at = (
-            (own_x, t, top),
-            (own_x, t, low),
-            (own_y, t, top),
-            (own_y, t, low),
-            (own_d, t, top),
-            (own_d, t, low),
-            (own, 1 - t, pl.ds(0, half)),
-            (own_x, 1 - t, top),
-            (own_x, 1 - t, low),
-            (own_y, 1 - t, top),
-            (own_y, 1 - t, low),
-            (own_d, 1 - t, top),
-            (own_d, 1 - t, low),
-        )[role]
-        view = nbuf.at[seq, side_at, at, :]
-        remote(view, view, g_send.at[role], g_recv.at[role], t_dev).wait_recv()
+        if role == 6:
+            view = nbuf.at[:, 1 - t]
+        else:
+            seq, at = (
+                (own_x, top),
+                (own_x, low),
+                (own_y, top),
+                (own_y, low),
+                (own_d, top),
+                (own_d, low),
+            )[role]
+            view = nbuf.at[seq, t, at, :]
+        remote(view, view, g_send.at[0], g_recv.at[role], t_dev).wait_recv()
 
     def gather_start(phase):
         for role in (1, 2, 0, 3, 6):
@@ -426,10 +429,9 @@
         rows_copy(phase, 11).start()
         rows_wait(phase, 5)
         rows_copy(phase, 12).start()
-        for role in range(6, 13):
-            rows_wait(phase, role)
-        for role in range(13):
-            rows_copy(phase, role).wait_send()
+        rows_wait(phase, 6)
+        sent(nbuf.at[pl.ds(0, 2)], g_send.at[0])
+        sent(nbuf.at[pl.ds(0, 3), 0], g_send.at[1])
 
     def products(phase, p, left, weights, k, piece=(0, 4)):
         need(k, p, piece)
@@ -466,7 +468,7 @@
 
     def sum_sems(phase, p, number, piece):
         place = PIECES.index((p, piece[0])) if phase else p
-        return m_send.at[place, number], m_recv.at[4 * phase + place, number]
+        return m_send.at[place, min(number, 1)], m_recv.at[4 * phase + place, number]
 
     def direct_copy(p, number, piece):
         at, device = span_of(piece), (x_dev, y_dev, d_dev)[number]
@@ -509,6 +511,11 @@
         start = pl.multiple_of((plane * 4 + piece[0]) * unit, unit)
         return pl.ds(start, piece[1] * unit)
 
+    def sums_sent(phase, p, piece):
+        sum_copies(phase, p, 0, piece).wait_send()
+        view = oth.at[p, pl.ds(0, 3), :, span_of(piece)]
+        sent(view, sum_sems(phase, p, 1, piece)[0])
+
     def last_sums(phase, p, base, piece):
         at, inside = columns_of(planes[p], piece), span_of(piece)
         if piece[1] == 1:
@@ -517,9 +524,7 @@
                 direct_copy(p, number, piece).wait_recv()
                 total = total + rd[piece[0] % 2, number].astype(F32)
             value = (base[:, at].astype(F32) + total).astype(LOW)
-            sum_copies(phase, p, 0, piece).wait_send()
-            for number in range(3):
-                direct_copy(p, number, piece).wait_send()
+            sums_sent(phase, p, piece)
             return at, [value[:part], value[part:]]
         values = []
         for i, number in enumerate((3, 4)):
@@ -527,8 +532,7 @@
             sum_copies(phase, p, number, piece).wait_recv()
             value = kept[p, r, y, span, inside].astype(F32) + r2[phase, p, i, :, inside].astype(F32)
             values.append((base[span, at].astype(F32) + value).astype(LOW))
-        for number in range(5):
-            sum_copies(phase, p, number, piece).wait_send()
+        sums_sent(phase, p, piece)
         return at, values
 
     def mix_done(p):
@@ -538,8 +542,8 @@
 
     def out_copy(p, piece):
         at = columns_of(lax.rem(planes[p], 2), piece)
-        src, place = oo.at[p, :, span_of(piece)], PIECES.index((p, piece[0]))
-        return remote(src, out.at[t, :, at], o_send.at[place], o_recv.at[place], t_dev)
+        src = oo.at[p, :, span_of(piece)]
+        return remote(src, out.at[t, :, at], o_sem.at[0], o_sem.at[1], t_dev)
 
     def down_done(p, piece=(0, 4)):
         _, values = last_sums(1, p, mx, piece)
@@ -557,21 +561,19 @@
                 oo[p, i * part : (i + 1) * part, span_of(piece)] = value
             out_copy(p, piece).start()
 
-    for i in range(2):
-        loads["rec", i].wait()
+    loaded(REC, f_rec)
     y_rec[...] = f_rec[1].astype(LOW)
     rec_w[f] = f_rec[0].astype(LOW)
-    pl.semaphore_wait(barrier, len(peers))
+    pl.semaphore_wait(barrier, 6)
     token_swap.start()
     y_copy(REC).start()
     send_own(REC, 0)
-    loads["tok"].wait()
+    loaded(4, tk.at[:, side])
     token_swap.wait()
     norm_rows(tk, gain_one)
     gather_start(0)
 
-    for i in range(2):
-        loads["mix", i].wait()
+    loaded(MIX, f_mix)
     y_mix[...] = (f_mix[1] * mix_scale[...]).astype(LOW)
     mix_w[f] = (f_mix[0] * mix_scale[...]).astype(LOW)
 
@@ -585,14 +587,13 @@
         lanes = slice(i * block, (i + 1) * block)
         ext[own, :, lanes] = jnp.broadcast_to(extra[i : i + 1, :], (ext.shape[1], block))
     ext_copies = [
-        remote(ext.at[own], ext.at[own], ex_send.at[i], ex_recv.at[i], device)
-        for i, device in enumerate((x_dev, y_dev, d_dev))
+        remote(ext.at[own], ext.at[own], ex_sem.at[0], ex_sem.at[1], device)
+        for device in (x_dev, y_dev, d_dev)
     ]
     for copy in ext_copies:
         copy.start()
-    for i in range(2):
-        for name in ("gate", "up", "down"):
-            loads[name, i].wait()
+    loaded(GU, f_gu)
+    loaded(DOWN, f_down)
     for i in range(2):
         y_gu[:, i * units : (i + 1) * units] = f_gu[1, i].astype(LOW)
         gu_w[f, :, i * units : (i + 1) * units] = f_gu[0, i].astype(LOW)
@@ -617,12 +618,12 @@
     forward(MIX, 0, 0)
     forward(MIX, 1, 0)
     gather_last(0)
-    for i, seq in enumerate((own_x, own_y, own_d)):
-        remote(ext.at[seq], ext.at[seq], ex_send.at[i], ex_recv.at[i], t_dev).wait_recv()
+    three = ext.at[pl.ds(0, 3)]
+    remote(three, three, ex_sem.at[0], ex_sem.at[1], t_dev).wait_recv()
     for p in range(1, 4):
         need(REC, p)
-    loads["recur"].wait()
-    loads["input"].wait()
+    loaded(5, recur_blocks)
+    loaded(6, input_blocks)
 
     at_chans = pl.multiple_of(q * chans, chans)
 
@@ -771,32 +772,17 @@
     down_done(3, third)
     down_done(3, fourth)
 
-    for p, piece in ((0, (0, 4)), (1, (0, 4)), (2, first), (2, second), (3, first), (3, third), (3, fourth)):
-        local = lax.div(planes[p], 2) == t
-
-        @pl.when(local)
-        def _():
-            out_copy(p, piece).wait_recv()
-
-        @pl.when(jnp.logical_not(local))
-        def _():
-            out_copy(p, piece).wait_send()
-
+    theirs_here = out.at[1 - t]
+    remote(theirs_here, theirs_here, o_sem.at[0], o_sem.at[1], t_dev).wait()
     for k in range(4):
         y_copy(k).wait_send()
-        for j in range(2):
-            for i, device in enumerate(near):
-                block_copy(k, own_place(k, j), wo_send.at[k, j, i], device).wait_send()
+        sent(mats[k].at[pl.ds(0, 4)], wo_send.at[k])
 
         @pl.when(inner)
         def _():
-            for far in range(2):
-                for j in range(2):
-                    for copy in forward_copies(k, far, j)[1]:
-                        copy.wait_send()
-
-    for copy in ext_copies:
-        copy.wait_send()
+            sent(mats[k].at[pl.ds(0, 4)], wf_send.at[k])
+
+    sent(ext.at[pl.ds(0, 3)], ex_sem.at[0])
 
 
 def team_body(
@@ -874,22 +860,19 @@
             vmem((4, half, 2 * cols), LOW),
             vmem((chans // block, block, block), LOW),
             vmem((chans // block, block, block), LOW),
-            dma((13,)),
+            dma((7,)),
+            dma((2,)),
+            dma((4,)),
+            dma((4,)),
+            dma((4,)),
+            dma((4, planes)),
+            dma((2,)),
+            dma((7,)),
             dma((2,)),
             dma((2,)),
-            dma((4,)),
-            dma((4, 2, 2)),
-            dma((4, 2, 2)),
-            dma((4, planes)),
-            dma((13,)),
-            dma((13,)),
+            dma((len(PIECES), 2)),
+            dma((4 + len(PIECES), 5)),
             dma((2,)),
-            dma((3,)),
-            dma((3,)),
-            dma((len(PIECES), 5)),
-            dma((4 + len(PIECES), 5)),
-            dma((len(PIECES),)),
-            dma((len(PIECES),)),
         ],
         compiler_params=pltpu.CompilerParams(
             collective_id=0, has_side_effects=True, vmem_limit_bytes=VMEM_BYTES

time: 194 us -> 193 us (level)
  no operation moved by 1% of the time
where the time goes in v4:
time: 193 us; the launch traced here: 192 us
  Pallas kernels  192 us (99%)
    pallas_call x1, Pallas kernels, team_body(): pl.pallas_call(layer_kernel, out_shape=vmem((2, half, half_width), LOW),...  192 us

profile of v4, /device:TPU:0, one launch (start us, length us, event | category | flops | bytes accessed | tf_op | source)
XLA Modules:
  0.0 192.5 jit_solution(15659966136321500629)
XLA Ops:
  0.0 191.6 %shard_map.172 = bf16[2,192,1024]{2,1,0:T(8,128)(2,1)S(1)} custom-call(bf16[384,1024]{1,0:T(8,128)(2,1)} %tokens.1, f32[256,1536]{1,0:T(8,128)} %w_rec.1, f32[1536,256]{1,0:T(8,128)} %w_mix.1, f32[256,2560]{1,0:T(8,128)} %w_gate.1, f32[256,2560]{1,0:T(8,128)} %w_up.1, f32[2560,256]{1,0:T(8,128)} %w_down.1, f32[1,2048]{1,0:T(1,128)} %bitcast.13, ...), custom_call_target="tpu_custom_call" | custom-call | tf_op jit(solution)/shard_map/pallas_call | solution.py:828
  191.6 0.9 copy.20

commit v5 on v4

--- a/solution.py
+++ b/solution.py
@@ -204,6 +204,8 @@
     r1,
     r2,
     rd,
+    rc,
+    base_rows,
     oo,
     recur_blocks,
     input_blocks,
@@ -220,6 +222,8 @@
     m_send,
     m_recv,
     o_sem,
+    c_send,
+    c_recv,
 ):
     rows, half_width = tokens.shape
     half, part = rows // 2, rows // 4
@@ -252,6 +256,9 @@
 
     for device in (x_dev, y_dev, t_dev, d_dev, near[0]):
         greet(device)
+
+    for device in (x_dev, y_dev, d_dev):
+        greet({**device, "tp": 1 - t})
 
     @pl.when(inner)
     def _():
@@ -476,6 +483,51 @@
         src, dst = kept.at[p, a, b, :, at], rd.at[piece[0] % 2, number]
         return remote(src, dst, *sum_sems(1, p, 1 + number, piece), device)
 
+    holder = lax.div(planes[3], 2)
+    collects = t == holder
+
+    def collect_copy(number):
+        a, b = ((1 - r, y), (r, 1 - y), (1 - r, 1 - y), (r, y))[number]
+        device = {**(x_dev, y_dev, d_dev, {})[number], "tp": holder}
+        if number == 3:
+            device = t_dev
+        send = c_send.at[0] if number == 3 else sum_sems(1, 3, 1, (3, 1))[0]
+        src = kept.at[3, a, b, :, span_of((3, 1))]
+        return remote(src, rc.at[t, number], send, c_recv.at[t, number], device)
+
+    def base_copy():
+        src = mx.at[:, columns_of(planes[3], (3, 1))]
+        return remote(src, base_rows, c_send.at[1], c_send.at[2], t_dev)
+
+    def collected(side, number):
+        view = rc.at[side, number]
+        remote(view, view, c_send.at[0], c_recv.at[side, number], t_dev).wait_recv()
+        return rc[side, number].astype(F32)
+
+    def collect_done():
+        piece = (3, 1)
+        at = columns_of(lax.rem(planes[3], 2), piece)
+
+        @pl.when(collects)
+        def _():
+            total = kept[3, r, y, :, span_of(piece)].astype(F32)
+            for number in range(3):
+                total = total + collected(t, number)
+            base = mx[:, columns_of(planes[3], piece)].astype(F32)
+            out[t, :, at] = (base + total).astype(LOW)
+            base_copy().wait_recv()
+            total = collected(1 - t, 3)
+            for number in range(3):
+                total = total + collected(1 - t, number)
+            out[1 - t, :, at] = (base_rows[...].astype(F32) + total).astype(LOW)
+
+        @pl.when(jnp.logical_not(collects))
+        def _():
+            collect_copy(3).wait_send()
+            base_copy().wait_send()
+
+        sums_sent(1, 3, piece)
+
     def pair_sums(phase, p, piece=(0, 4)):
         sum_copies(phase, p, 0, piece).wait_recv()
         at = span_of(piece)
@@ -487,7 +539,11 @@
             return carry
 
         lax.fori_loop(0, 4, step, 0)
-        if piece[1] == 1:
+        if piece == (3, 1):
+            for number in (2, 0, 1):
+                collect_copy(number).start()
+            pl.when(jnp.logical_not(collects))(lambda: collect_copy(3).start())
+        elif piece[1] == 1:
             for number in (2, 0, 1):
                 direct_copy(p, number, piece).start()
         else:
@@ -564,7 +620,7 @@
     loaded(REC, f_rec)
     y_rec[...] = f_rec[1].astype(LOW)
     rec_w[f] = f_rec[0].astype(LOW)
-    pl.semaphore_wait(barrier, 6)
+    pl.semaphore_wait(barrier, 9)
     token_swap.start()
     y_copy(REC).start()
     send_own(REC, 0)
@@ -707,6 +763,7 @@
 
     norm_rows(mx, gain_two)
     gather_start(1)
+    pl.when(jnp.logical_not(collects))(lambda: base_copy().start())
     gather_first(1)
     wait_block(DOWN, fp)
     forward(GU, 0, 1)
@@ -770,10 +827,22 @@
     pair_sums(1, 3, fourth)
     down_done(3, first)
     down_done(3, third)
-    down_done(3, fourth)
-
-    theirs_here = out.at[1 - t]
-    remote(theirs_here, theirs_here, o_sem.at[0], o_sem.at[1], t_dev).wait()
+    collect_done()
+
+    whole, less = out.at[1 - t], out.at[1 - t, :, pl.ds(0, half_width - unit)]
+    whole = remote(whole, whole, o_sem.at[0], o_sem.at[1], t_dev)
+    less = remote(less, less, o_sem.at[0], o_sem.at[1], t_dev)
+
+    @pl.when(collects)
+    def _():
+        less.wait_recv()
+        whole.wait_send()
+
+    @pl.when(jnp.logical_not(collects))
+    def _():
+        whole.wait_recv()
+        less.wait_send()
+
     for k in range(4):
         y_copy(k).wait_send()
         sent(mats[k].at[pl.ds(0, 4)], wo_send.at[k])
@@ -857,6 +926,8 @@
             vmem((2, 4, 2, 2, part, 2 * cols), LOW),
             vmem((2, 4, 2, part, 2 * cols), LOW),
             vmem((2, 3, half, cols // 2), LOW),
+            vmem((2, 4, half, cols // 2), LOW),
+            vmem((half, cols // 2), LOW),
             vmem((4, half, 2 * cols), LOW),
             vmem((chans // block, block, block), LOW),
             vmem((chans // block, block, block), LOW),
@@ -873,6 +944,8 @@
             dma((len(PIECES), 2)),
             dma((4 + len(PIECES), 5)),
             dma((2,)),
+            dma((3,)),
+            dma((2, 4)),
         ],
         compiler_params=pltpu.CompilerParams(
             collective_id=0, has_side_effects=True, vmem_limit_bytes=VMEM_BYTES

time: 193 us -> 192 us (level)
  Pallas kernels: 192 us -> 190 us
where the time goes in v5:
time: 192 us; the launch traced here: 191 us
  Pallas kernels  190 us (99%)
    pallas_call x1, Pallas kernels, team_body(): pl.pallas_call(layer_kernel, out_shape=vmem((2, half, half_width), LOW),...  190 us

profile of v5, /device:TPU:0, one launch (start us, length us, event | category | flops | bytes accessed | tf_op | source)
XLA Modules:
  0.0 191.2 jit_solution(2281215678399959551)
XLA Ops:
  0.0 190.3 %shard_map.172 = bf16[2,192,1024]{2,1,0:T(8,128)(2,1)S(1)} custom-call(bf16[384,1024]{1,0:T(8,128)(2,1)} %tokens.1, f32[256,1536]{1,0:T(8,128)} %w_rec.1, f32[1536,256]{1,0:T(8,128)} %w_mix.1, f32[256,2560]{1,0:T(8,128)} %w_gate.1, f32[256,2560]{1,0:T(8,128)} %w_up.1, f32[2560,256]{1,0:T(8,128)} %w_down.1, f32[1,2048]{1,0:T(1,128)} %bitcast.13, ...), custom_call_target="tpu_custom_call" | custom-call | tf_op jit(solution)/shard_map/pallas_call | solution.py:897
  190.3 0.9 copy.20

commit v6 on v5

--- a/solution.py
+++ b/solution.py
@@ -475,7 +475,7 @@
 
     def sum_sems(phase, p, number, piece):
         place = PIECES.index((p, piece[0])) if phase else p
-        return m_send.at[place, min(number, 1)], m_recv.at[4 * phase + place, number]
+        return m_send.at[place, min(number, 1)], m_recv.at[place, number]
 
     def direct_copy(p, number, piece):
         at, device = span_of(piece), (x_dev, y_dev, d_dev)[number]
@@ -942,7 +942,7 @@
             dma((2,)),
             dma((2,)),
             dma((len(PIECES), 2)),
-            dma((4 + len(PIECES), 5)),
+            dma((len(PIECES), 5)),
             dma((2,)),
             dma((3,)),
             dma((2, 4)),

time: 192 us -> 192 us (level)
  no operation moved by 1% of the time
where the time goes in v6:
time: 192 us; the launch traced here: 191 us
  Pallas kernels  190 us (99%)
    pallas_call x1, Pallas kernels, team_body(): pl.pallas_call(layer_kernel, out_shape=vmem((2, half, half_width), LOW),...  190 us

profile of v6, /device:TPU:0, one launch (start us, length us, event | category | flops | bytes accessed | tf_op | source)
XLA Modules:
  0.0 191.0 jit_solution(10615859499899599891)
XLA Ops:
  0.0 190.1 %shard_map.172 = bf16[2,192,1024]{2,1,0:T(8,128)(2,1)S(1)} custom-call(bf16[384,1024]{1,0:T(8,128)(2,1)} %tokens.1, f32[256,1536]{1,0:T(8,128)} %w_rec.1, f32[1536,256]{1,0:T(8,128)} %w_mix.1, f32[256,2560]{1,0:T(8,128)} %w_gate.1, f32[256,2560]{1,0:T(8,128)} %w_up.1, f32[2560,256]{1,0:T(8,128)} %w_down.1, f32[1,2048]{1,0:T(1,128)} %bitcast.13, ...), custom_call_target="tpu_custom_call" | custom-call | tf_op jit(solution)/shard_map/pallas_call | solution.py:897
  190.1 0.9 copy.20
